TPU v7x, 32 devices: a whole 2x2x4 slice. The times are simulated.
32 devices in a mesh: sp: 8 (over z, y), tp: 4 (over x, core).
Axes of the slice: x: 2, y: 2, z: 4, core: 2. Of those that a mesh axis runs over, the one named last changes fastest.
Arguments:
- resid_in: bfloat16 [1024, 2048], P('sp'), may hold values from -6 to 6
- query_plain: bfloat16 [1024, 2048], P('sp', 'tp'), may hold values from -480 to 480, as said below
- query_turn: bfloat16 [1024, 1024], P('sp', 'tp'), may hold values from -16 to 16
- latent_raw: bfloat16 [1024, 256], P('sp'), may hold values from -6 to 6
- shared_key: bfloat16 [1024, 32], P('sp'), may hold values from -6 to 6
- latent_gain: float32 [256], replicated, may hold values from 0.1 to 1.9
- key_up: bfloat16 [256, 2048], P(None, 'tp'), may hold values from -0.375 to 0.375
- value_up: bfloat16 [256, 2048], P(None, 'tp'), may hold values from -0.375 to 0.375
- out_weight: bfloat16 [2048, 2048], P('tp'), may hold values from -0.5 to 0.5
- mixer_gain: float32 [2048], replicated, may hold values from 0.1 to 1.9
- gate_weight: bfloat16 [2048, 5632], P('sp', 'tp'), may hold values from -0.125 to 0.125
- up_weight: bfloat16 [2048, 5632], P('sp', 'tp'), may hold values from -0.125 to 0.125
- down_weight: bfloat16 [5632, 2048], P('tp', 'sp'), may hold values from -0.15625 to 0.15625
Outputs:
- layer_out: bfloat16 [1024, 2048], P(('sp', 'tp'))
Inputs may be any that keep to these rules, and one draw needn't show every extreme that they name: Entries of query_plain lie in this range.
All inputs are finite; a program needn't handle non-finite values.
Results may differ from a plain program's by a relative error of at most 0.014.
The roundings to bfloat16 on the way count: a program that leaves them out, or rounds other values in their place, can miss the bound.
Values may be sent and summed in bfloat16 or wider, within the bound.
A program may use at most 128 MiB of HBM per device.

v0:
```python
import functools
import math

import jax
import jax.numpy as jnp
from jax import lax
from jax.experimental import pallas as pl
from jax.experimental.pallas import tpu as pltpu
from jax.sharding import PartitionSpec as P

NOPE = 64
ROPE = 32
V = 64


def rotate(values, cosine, sine):
    half_width = values.shape[-1] // 2
    first = values[..., :half_width]
    second = values[..., half_width:]
    return jnp.concatenate(
        [first * cosine - second * sine, first * sine + second * cosine], axis=-1
    )


def rms_scale(values, gain):
    return values * lax.rsqrt(jnp.mean(values * values, axis=-1, keepdims=True) + 1e-06) * gain


def plain_layer(
    resid_in,
    query_plain,
    query_turn,
    latent_raw,
    shared_key,
    latent_gain,
    key_up,
    value_up,
    out_weight,
    mixer_gain,
    gate_weight,
    up_weight,
    down_weight,
):
    tok_rows = resid_in.shape[0]
    head_count = query_plain.shape[1] // NOPE
    part_rows = tok_rows // lax.axis_size("tp")
    offset = lax.axis_index("sp") * tok_rows
    position = (offset + jnp.arange(tok_rows, dtype=jnp.int32)).astype(jnp.float32)
    inverse = 10000.0 ** (-jnp.arange(0, ROPE, 2, dtype=jnp.float32) / ROPE)
    angles = position[:, None] * inverse[None, :]
    cosine = jnp.cos(angles)
    sine = jnp.sin(angles)
    query_heads = query_plain.reshape(tok_rows, head_count, NOPE)
    query_rot = rotate(
        query_turn.reshape(tok_rows, head_count, ROPE).astype(jnp.float32),
        cosine[:, None, :],
        sine[:, None, :],
    ).astype(jnp.bfloat16)
    latent = rms_scale(latent_raw.astype(jnp.float32), latent_gain).astype(jnp.bfloat16)
    key_rot = rotate(shared_key.astype(jnp.float32), cosine, sine).astype(jnp.bfloat16)
    softmax_scale = (NOPE + ROPE) ** (-0.5)

    def attend_block(state, key_plain, values, key_pos):
        run_max, run_total, run_acc = state
        score = jnp.einsum(
            "qhd,khd->hqk", query_heads, key_plain, preferred_element_type=jnp.float32
        )
        score = score + jnp.einsum(
            "qhr,kr->hqk", query_rot, key_pos, preferred_element_type=jnp.float32
        )
        score = score * softmax_scale
        new_max = jnp.maximum(run_max, jnp.max(score, axis=-1))
        shrink = jnp.exp(run_max - new_max)
        expo = jnp.exp(score - new_max[:, :, None])
        run_total = run_total * shrink + jnp.sum(expo, axis=-1)
        run_acc = run_acc * shrink.T[:, :, None] + jnp.einsum(
            "hqk,khd->qhd", expo.astype(jnp.bfloat16), values, preferred_element_type=jnp.float32
        )
        return (new_max, run_total, run_acc)

    start_state = (
        jnp.full((head_count, tok_rows), -jnp.inf, jnp.float32),
        jnp.zeros((head_count, tok_rows), jnp.float32),
        jnp.zeros((tok_rows, head_count, V), jnp.float32),
    )
    state = start_state
    latent_piece = lax.all_gather(latent, "sp", axis=0, tiled=True)
    pos_piece = lax.all_gather(key_rot, "sp", axis=0, tiled=True)
    piece_len = latent_piece.shape[0]
    block_len = math.gcd(piece_len, 512)
    block_count = piece_len // block_len

    def one_block(inner, items):
        latent_rows, pos_rows = items
        key_plain = (
            jnp.dot(latent_rows, key_up, preferred_element_type=jnp.float32)
            .astype(jnp.bfloat16)
            .reshape(block_len, head_count, NOPE)
        )
        values = (
            jnp.dot(latent_rows, value_up, preferred_element_type=jnp.float32)
            .astype(jnp.bfloat16)
            .reshape(block_len, head_count, V)
        )
        return (attend_block(inner, key_plain, values, pos_rows), None)

    state, unused = lax.scan(
        one_block,
        state,
        (
            latent_piece.reshape(block_count, block_len, latent_piece.shape[1]),
            pos_piece.reshape(block_count, block_len, ROPE),
        ),
    )
    attended = (
        (state[2] / state[1].T[:, :, None]).astype(jnp.bfloat16).reshape(tok_rows, head_count * V)
    )
    own_start = lax.axis_index("tp") * part_rows
    mixed = lax.psum_scatter(
        jnp.dot(attended, out_weight, preferred_element_type=jnp.float32).astype(jnp.bfloat16),
        "tp",
        scatter_dimension=0,
        tiled=True,
    ).astype(jnp.float32)
    middle = lax.dynamic_slice_in_dim(resid_in, own_start, part_rows, 0).astype(jnp.float32) + mixed
    normed = rms_scale(middle, mixer_gain).astype(jnp.bfloat16)
    all_rows = lax.all_gather(normed, "tp", axis=0, tiled=True)
    gate_sum = jnp.dot(
        all_rows,
        lax.all_gather(gate_weight, "sp", axis=0, tiled=True),
        preferred_element_type=jnp.float32,
    )
    up_sum = jnp.dot(
        all_rows,
        lax.all_gather(up_weight, "sp", axis=0, tiled=True),
        preferred_element_type=jnp.float32,
    )
    hidden = (jax.nn.silu(gate_sum) * up_sum).astype(jnp.bfloat16)
    terms = jnp.dot(
        hidden,
        lax.all_gather(down_weight, "sp", axis=1, tiled=True),
        preferred_element_type=jnp.float32,
    )
    down_sum = lax.psum_scatter(
        terms.astype(jnp.bfloat16), "tp", scatter_dimension=0, tiled=True
    ).astype(jnp.float32)
    return (middle + 0.5 * down_sum).astype(jnp.bfloat16)

MESH = pl.DeviceIdType.MESH
BF = jnp.bfloat16
F32 = jnp.float32
BY_LAST = (((1,), (1,)), ((), ()))


def turn(values, cosine, sine):
    width = values.shape[-1]
    half = ROPE // 2
    lane = lax.broadcasted_iota(jnp.int32, values.shape, 1) % ROPE
    swapped = jnp.where(lane < half, pltpu.roll(values, width - half, 1), pltpu.roll(values, half, 1))
    return values * cosine + swapped * sine


def layer_kernel(
    sizes,
    resid_ref,
    query_ref,
    turn_ref,
    latent_ref,
    shared_ref,
    cos_ref,
    sin_ref,
    lgain_ref,
    kup_ref,
    vup_ref,
    ow_ref,
    mgain_ref,
    gate_ref,
    up_ref,
    down_ref,
    out_ref,
    kv_buf,
    key_buf,
    val_buf,
    att_buf,
    mix_buf,
    mixb_buf,
    mixr_buf,
    mid_buf,
    w_buf,
    n_buf,
    p_buf,
    r1_buf,
    acc_buf,
    r_buf,
    w_ssem,
    w_rsem,
    w_lsem,
    l_ssem,
    l_rsem,
    f_ssem,
    f_rsem,
    m_ssem,
    m_rsem,
    a_ssem,
    a_rsem,
    d_ssem,
    d_rsem,
    c_ssem,
    c_rsem,
    s_ssem,
    s_rsem,
):
    sp, tp, dims = sizes
    axes = range(len(dims))
    ring_dims, tp_dims = dims[:-1], dims[-1]
    s = lax.axis_index("sp")
    t = lax.axis_index("tp")
    core = t % 2
    other = t + 1 - 2 * core
    me = ()
    rest = s
    for size in reversed(ring_dims):
        me = (rest % size,) + me
        rest = rest // size
    me = me + (t // 2,)
    rows = latent_ref.shape[0]
    part = rows // tp
    hid, cols = gate_ref.shape[1:]
    kv_width = latent_ref.shape[1]

    def remote(src, dst, ssem, rsem, dev):
        return pltpu.make_async_remote_copy(
            src_ref=src, dst_ref=dst, send_sem=ssem, recv_sem=rsem, device_id=dev, device_id_type=MESH
        )

    sends = []

    lat = latent_ref[...].astype(F32)
    lat = lat * lax.rsqrt(jnp.mean(lat * lat, axis=-1, keepdims=True) + 1e-06) * lgain_ref[...]
    cosine = cos_ref[...]
    sine = sin_ref[...]
    half_rows = rows // 2
    own_lat = lat.astype(BF)
    own_key = turn(shared_ref[...].astype(F32), cosine, sine).astype(BF)
    for half in range(2):
        part_of = slice(half * half_rows, (half + 1) * half_rows)
        kv_buf[0, half, :, :kv_width] = own_lat[part_of]
        kv_buf[0, half, :, kv_width:] = own_key[part_of]
    for k in range(1, sp):
        cp = remote(kv_buf.at[0, core], kv_buf.at[k, core], l_ssem.at[k], l_rsem.at[k], ((s + k) % sp, t))
        cp.start()
        sends.append(cp)
    def index_of(place):
        index = 0
        for p, size in zip(place, dims):
            index = index * size + p
        return index

    def shifted(offset):
        return tuple((m + o) % n for m, o, n in zip(me, offset, dims))

    def device(offset):
        place = shifted(offset)
        ring = 0
        for p, size in zip(place, ring_dims):
            ring = ring * size + p
        return (ring, place[-1] * 2 + core)

    def along(d, k):
        return tuple(k if i == d else 0 for i in axes)

    def plus(offset, d, k):
        return tuple((o + k) % dims[d] if i == d else o for i, o in enumerate(offset))

    def offsets(sizes_of):
        found = [()]
        for size in sizes_of:
            found = [f + (k,) for f in found for k in range(size)]
        return found

    parts_of_w = (gate_ref, up_ref, down_ref)

    def w_slot(which):
        return w_buf.at[which * hid:(which + 1) * hid, pl.ds(pl.multiple_of(s * cols, cols), cols)]

    keeps = [
        pltpu.make_async_copy(ref.at[s], w_slot(which), w_lsem.at[which])
        for which, ref in enumerate(parts_of_w)
    ]
    for keep in keeps:
        keep.start()
    ring = sorted(offsets(ring_dims)[1:], reverse=True)
    late = [o for o in ring if o[0]][-2:] + ring[-3:]
    early = [o for o in ring if o not in late]

    def send_weights(some, out):
        for which, ref in enumerate(parts_of_w):
            for offset in some:
                dest = device(offset + (0,))
                i = index_of(offset + (0,)) // tp_dims
                cp = remote(
                    ref.at[dest[0]], w_slot(which), w_ssem.at[which, i], w_rsem.at[which, i], dest
                )
                cp.start()
                out.append(cp)

    send_weights(early, sends)

    def make_kv(k):
        piece = kv_buf[k].reshape(rows, kv_buf.shape[3])
        piece_lat = piece[:, :kv_width]
        key_buf[k * rows:(k + 1) * rows, :] = jnp.dot(
            piece_lat, kup_ref[...], preferred_element_type=F32
        ).astype(BF)
        val_buf[k * rows:(k + 1) * rows, :] = jnp.dot(
            piece_lat, vup_ref[...], preferred_element_type=F32
        ).astype(BF)

    make_kv(0)
    query_rot = turn(
        turn_ref[...].astype(F32),
        jnp.concatenate([cosine] * (turn_ref.shape[1] // cosine.shape[1]), axis=1),
        jnp.concatenate([sine] * (turn_ref.shape[1] // cosine.shape[1]), axis=1),
    ).astype(BF)
    for k in range(1, sp):
        remote(kv_buf.at[k, core], kv_buf.at[k, core], l_ssem.at[k], l_rsem.at[k], (s, other)).wait_recv()
        cp = remote(kv_buf.at[k, core], kv_buf.at[k, core], f_ssem.at[k], f_rsem.at[k], (s, other))
        cp.start()
        sends.append(cp)
    for k in range(1, sp):
        remote(
            kv_buf.at[k, 1 - core], kv_buf.at[k, 1 - core], f_ssem.at[k], f_rsem.at[k], (s, other)
        ).wait_recv()
        make_kv(k)

    scale = (NOPE + ROPE) ** (-0.5)
    all_rot = kv_buf[...].reshape(sp * rows, kv_buf.shape[3])[:, kv_width:]
    lane = lax.broadcasted_iota(jnp.int32, (rows, 128), 1)
    for pair in range(query_ref.shape[1] // 128):
        span = slice(pair * 128, (pair + 1) * 128)
        keys = jnp.concatenate([key_buf[:, span], all_rot], axis=1)
        vals = val_buf[:, span]
        results = []
        for inner in range(2):
            head = pair * 2 + inner
            tile = head * ROPE // 128
            group = head % (128 // ROPE)
            q_plain = jnp.where(lane // NOPE == inner, query_ref[:, span], jnp.zeros((), BF))
            q_turn = jnp.where(
                lane // ROPE == group, query_rot[:, tile * 128:(tile + 1) * 128], jnp.zeros((), BF)
            )
            score = lax.dot_general(
                jnp.concatenate([q_plain, q_turn], axis=1), keys, BY_LAST, preferred_element_type=F32
            ) * scale
            top = jnp.max(score, axis=-1, keepdims=True)
            expo = jnp.exp(score - top)
            total = jnp.sum(expo, axis=-1, keepdims=True)
            results.append(jnp.dot(expo.astype(BF), vals, preferred_element_type=F32) / total)
        att_buf[:, span] = jnp.where(lane < V, results[0], results[1]).astype(BF)

    mix_buf[...] = jnp.dot(att_buf[...], ow_ref[...], preferred_element_type=F32)
    mixb_buf[...] = mix_buf[...].astype(BF).reshape(mixb_buf.shape)
    for j in range(1, tp):
        dest = (t + j) % tp
        cp = remote(mixb_buf.at[dest], mixr_buf.at[j], m_ssem.at[j], m_rsem.at[j], (s, dest))
        cp.start()
        sends.append(cp)
    own_rows = pl.ds(pl.multiple_of(t * part, part), part)
    mid = resid_ref[own_rows, :].astype(F32) + mix_buf[own_rows, :]
    for j in range(1, tp):
        remote(mixb_buf.at[0], mixr_buf.at[j], m_ssem.at[j], m_rsem.at[j], (s, other)).wait_recv()
        mid = mid + mixr_buf[j].astype(F32)
    mid_buf[...] = mid
    normed = mid * lax.rsqrt(jnp.mean(mid * mid, axis=-1, keepdims=True) + 1e-06) * mgain_ref[...]
    mine = index_of(me)
    n_buf[mine, core] = normed.astype(BF)

    def gather(order):
        held = [((0,) * len(dims), -1)]
        out = []
        for stage, d in enumerate(order):
            for offset, _ in list(held):
                for k in range(1, dims[d]):
                    held.append((plus(offset, d, k), stage))
        for offset, stage in held:
            block = n_buf.at[index_of(shifted(offset)), core]
            if stage >= 0:
                i = index_of(offset)
                remote(block, block, a_ssem.at[i], a_rsem.at[i], (s, other)).wait_recv()
            for d in order[stage + 1:]:
                for k in range(1, dims[d]):
                    i = index_of(plus(offset, d, -k))
                    cp = remote(block, block, a_ssem.at[i], a_rsem.at[i], device(along(d, k)))
                    cp.start()
                    out.append(cp)
            i = index_of(offset)
            cp = remote(block, block, d_ssem.at[i], d_rsem.at[i], (s, other))
            cp.start()
            out.append(cp)
            if stage == 0:
                send_weights(late, out)
        for offset, _ in held:
            i = index_of(offset)
            block = n_buf.at[index_of(shifted(offset)), 1 - core]
            remote(block, block, d_ssem.at[i], d_rsem.at[i], (s, other)).wait_recv()
        for cp in out:
            cp.wait_send()

    def feed_forward(order):
        def arrived(which):
            keeps[which].wait()
            piece = w_buf.at[which * hid:(which + 1) * hid, :cols]
            for i in range(1, sp):
                remote(piece, piece, w_ssem.at[which, i], w_rsem.at[which, i], (s, other)).wait_recv()

        arrived(0)
        arrived(1)
        out = []
        zero = (0,) * len(dims)
        inner = offsets(dims[2:])
        step = len(inner)
        chunks = sorted(offsets(dims[:2]), key=lambda o: (o[1] == 0, o[0] == 0))

        def send(offset, d):
            i = index_of(plus(plus(offset, d, -offset[d]), d, -offset[d]))
            cp = remote(
                acc_buf.at[index_of(shifted(offset))], r_buf.at[i], s_ssem.at[i], s_rsem.at[i],
                device(along(d, offset[d])),
            )
            cp.start()
            out.append(cp)

        def across(g, outer):
            base = index_of(shifted(outer + zero[2:])[:2] + zero[2:])
            some = pl.ds(base, step)
            return some, remote(
                p_buf.at[some, 1 - core], r1_buf.at[some], c_ssem.at[g], c_rsem.at[g], (s, other)
            )

        def join(g, outer):
            some, cp = across(g, outer)
            cp.wait()
            acc_buf[some] = (p_buf[some, core].astype(F32) + r1_buf[some].astype(F32)).astype(BF)
            for o in inner:
                if (outer + o)[order[0]]:
                    send(outer + o, order[0])

        for g, outer in enumerate(chunks):
            some, cp = across(g, outer)
            block = n_buf[some].reshape(step * 2 * part, n_buf.shape[3])
            gate = lax.dot_general(block, w_buf[:hid], BY_LAST, preferred_element_type=F32)
            up = lax.dot_general(block, w_buf[hid:2 * hid], BY_LAST, preferred_element_type=F32)
            hidden = (gate / (1.0 + jnp.exp(-gate)) * up).astype(BF)
            if g == 0:
                arrived(2)
            down = jnp.dot(hidden, w_buf[2 * hid:], preferred_element_type=F32)
            p_buf[some] = down.astype(BF).reshape(step, 2, part, n_buf.shape[3])
            cp.start()
            if g:
                join(g - 1, chunks[g - 1])
        join(len(chunks) - 1, chunks[-1])

        live = [outer + o for outer in chunks for o in inner]
        for stage, d in enumerate(order):
            last = stage == len(order) - 1
            live = [o for o in live if o[d] == 0]
            if not last:
                live = [o for o in live if o[order[stage + 1]]] + [o for o in live if not o[order[stage + 1]]]
            for offset in live:
                b = index_of(shifted(offset))
                value = acc_buf[b].astype(F32)
                for k in range(1, dims[d]):
                    i = index_of(plus(offset, d, k))
                    remote(r_buf.at[i], r_buf.at[i], s_ssem.at[i], s_rsem.at[i], (s, other)).wait_recv()
                    value = value + r_buf[i].astype(F32)
                if last:
                    out_ref[...] = (mid_buf[...] + 0.5 * value).astype(BF)
                else:
                    acc_buf[b] = value.astype(BF)
                    if offset[order[stage + 1]]:
                        send(offset, order[stage + 1])
        for cp in out:
            cp.wait_send()

    @pl.when(core == 0)
    def _():
        gather((0, 1, 2, 3))
        feed_forward((3, 2, 1, 0))

    @pl.when(core == 1)
    def _():
        gather((0, 1, 2, 3))
        feed_forward((2, 3, 1, 0))

    for cp in sends:
        cp.wait_send()


def fused_layer(
    resid_in,
    query_plain,
    query_turn,
    latent_raw,
    shared_key,
    latent_gain,
    key_up,
    value_up,
    out_weight,
    mixer_gain,
    gate_weight,
    up_weight,
    down_weight,
):
    sp = lax.axis_size("sp")
    tp = lax.axis_size("tp")
    dims = (2, sp // 4, 2, tp // 2)
    rows, width = resid_in.shape
    part = rows // tp
    hid = down_weight.shape[0] // sp
    cols = down_weight.shape[1]
    kv = latent_raw.shape[1]
    heads_width = query_plain.shape[1]
    position = (lax.axis_index("sp") * rows + jnp.arange(rows, dtype=jnp.int32)).astype(F32)
    inverse = 10000.0 ** (-jnp.arange(0, ROPE, 2, dtype=F32) / ROPE)
    inverse_lanes = jnp.tile(inverse, 128 * 2 // ROPE)
    angles = position[:, None] * inverse_lanes[None, :]
    sign = jnp.where(jnp.arange(128) % ROPE < ROPE // 2, -1.0, 1.0).astype(F32)
    cosine = jnp.cos(angles)
    sine = jnp.sin(angles) * sign[None, :]
    groups = sp * tp // 2
    chunks = dims[0] * dims[1]
    dma = pltpu.SemaphoreType.DMA
    vmem = lambda *shape: pltpu.VMEM(shape, BF)
    return pl.pallas_call(
        functools.partial(layer_kernel, (sp, tp, dims)),
        out_shape=jax.ShapeDtypeStruct((part, width), BF),
        in_specs=[pl.BlockSpec(memory_space=pltpu.VMEM)] * 15,
        out_specs=pl.BlockSpec(memory_space=pltpu.VMEM),
        scratch_shapes=[
            vmem(sp, 2, rows // 2, kv + 128),
            vmem(sp * rows, heads_width),
            vmem(sp * rows, heads_width),
            vmem(rows, heads_width),
            pltpu.VMEM((rows, width), F32),
            vmem(tp, part, width),
            vmem(tp, part, width),
            pltpu.VMEM((part, width), F32),
            vmem(3 * hid, width),
            vmem(groups, 2, part, width),
            vmem(groups, 2, part, width),
            vmem(groups, part, width),
            vmem(groups, part, width),
            vmem(groups, part, width),
            dma((3, sp)),
            dma((3, sp)),
            dma((3,)),
            dma((sp,)),
            dma((sp,)),
            dma((sp,)),
            dma((sp,)),
            dma((tp,)),
            dma((tp,)),
            dma((groups,)),
            dma((groups,)),
            dma((groups,)),
            dma((groups,)),
            dma((chunks,)),
            dma((chunks,)),
            dma((groups,)),
            dma((groups,)),
        ],
        compiler_params=pltpu.CompilerParams(has_side_effects=True, vmem_limit_bytes=60 * 1024 * 1024),
    )(
        resid_in,
        query_plain,
        query_turn,
        latent_raw,
        jnp.tile(shared_key, (1, 128 // ROPE)),
        cosine,
        sine,
        latent_gain[None, :],
        key_up,
        value_up,
        out_weight,
        mixer_gain[None, :],
        gate_weight.T.reshape(sp, hid, cols),
        up_weight.T.reshape(sp, hid, cols),
        down_weight.reshape(sp, hid, cols),
    )


def per_device(*arrays):
    resid_in, query_plain, query_turn, latent_raw = arrays[:4]
    down_weight = arrays[-1]
    sp = lax.axis_size("sp")
    tp = lax.axis_size("tp")
    rows = resid_in.shape[0]
    fits = (
        sp % 4 == 0
        and tp % 2 == 0
        and rows % (32 * tp) == 0
        and down_weight.shape[0] % (16 * sp) == 0
        and down_weight.shape[1] % 128 == 0
        and latent_raw.shape[1] % 128 == 0
        and query_plain.shape[1] % 128 == 0
        and query_turn.shape[1] % 128 == 0
        and rows * sp <= 1024
        and sp * tp <= 32
    )
    if fits:
        return fused_layer(*arrays)
    return plain_layer(*arrays)


def solution(mesh):
    return jax.shard_map(
        per_device,
        mesh=mesh,
        in_specs=(
            P("sp", None),
            P("sp", "tp"),
            P("sp", "tp"),
            P("sp", None),
            P("sp", None),
            P(),
            P(None, "tp"),
            P(None, "tp"),
            P("tp", None),
            P(),
            P("sp", "tp"),
            P("sp", "tp"),
            P("tp", "sp"),
        ),
        out_specs=P(("sp", "tp"), None),
        check_vma=False,
    )
```

profile of v0, /device:TPU:0, one launch (start us, length us, event | category | flops | bytes accessed | tf_op | source)
XLA Modules:
  0.0 126.7 jit_solution(2003506338798271580)
XLA Ops:
  0.0 0.0 copy-start
  0.0 0.1 mul.36
  0.1 0.8 tile.6
  0.9 0.7 copy.19.shared_ref
  1.6 1.0 fusion
  2.6 2.2 %copy.17 = bf16[1408,256]{1,0:T(8,128)(2,1)} copy(bf16[1408,256]{0,1:T(8,128)(2,1)} %bitcast.11) | data formatting | bytes 1441792 | tf_op jit(solution)/shard_map/transpose | solution.py:586
  4.8 0.0 copy-done
  4.8 1.1 copy.18
  6.0 119.2 %shard_map.127 = bf16[32,2048]{1,0:T(8,128)(2,1)} custom-call(bf16[128,2048]{1,0:T(8,128)(2,1)} %resid_ref.1, bf16[128,512]{1,0:T(8,128)(2,1)} %query_ref.1, bf16[128,256]{1,0:T(8,128)(2,1)} %turn_ref.1, bf16[128,256]{1,0:T(8,128)(2,1)} %latent_ref.1, bf16[128,128]{1,0:T(8,128)(2,1)} %copy.19.shared_ref, f32[128,128]{1,0:T(8,128)} %get-tuple-element.6.cos_ref, ...), custom_call_target="tpu_custom_call" | custom-call | tf_op jit(solution)/shard_map/pallas_call | solution.py:534
  125.2 1.6 %copy.21 = bf16[32,2048]{1,0:T(8,128)(2,1)} copy(bf16[32,2048]{1,0:T(8,128)(2,1)} %shard_map.127) | data formatting | bytes 262144
  (4 shorter events, 0.0 us)
Async XLA Ops:
  0.0 4.8 %copy-start = (bf16[256,1408]{1,0:T(8,128)(2,1)S(1)}, bf16[256,1408]{1,0:T(8,128)(2,1)}, u32[]{:S(2)}) copy-start(bf16[256,1408]{1,0:T(8,128)(2,1)} %param.24) | copy-start | bytes 2162692
where the time goes:
time: 127 us
  Pallas kernels  119 us (94%)
  local copies, waits for them, and re-layouts  6.52 us (5%)
    pallas_call x1, Pallas kernels, fused_layer(): pl.pallas_call(functools.partial(layer_kernel, (sp, tp, dims)), out_shape...  119 us

commit v1 on v0

v1 whole, which is shorter than its diff:
```python
import functools
import math

import jax
import jax.numpy as jnp
from jax import lax
from jax.experimental import pallas as pl
from jax.experimental.pallas import tpu as pltpu
from jax.sharding import PartitionSpec as P

NOPE = 64
ROPE = 32
V = 64


def rotate(values, cosine, sine):
    half_width = values.shape[-1] // 2
    first = values[..., :half_width]
    second = values[..., half_width:]
    return jnp.concatenate(
        [first * cosine - second * sine, first * sine + second * cosine], axis=-1
    )


def rms_scale(values, gain):
    return values * lax.rsqrt(jnp.mean(values * values, axis=-1, keepdims=True) + 1e-06) * gain


def plain_layer(
    resid_in,
    query_plain,
    query_turn,
    latent_raw,
    shared_key,
    latent_gain,
    key_up,
    value_up,
    out_weight,
    mixer_gain,
    gate_weight,
    up_weight,
    down_weight,
):
    tok_rows = resid_in.shape[0]
    head_count = query_plain.shape[1] // NOPE
    part_rows = tok_rows // lax.axis_size("tp")
    offset = lax.axis_index("sp") * tok_rows
    position = (offset + jnp.arange(tok_rows, dtype=jnp.int32)).astype(jnp.float32)
    inverse = 10000.0 ** (-jnp.arange(0, ROPE, 2, dtype=jnp.float32) / ROPE)
    angles = position[:, None] * inverse[None, :]
    cosine = jnp.cos(angles)
    sine = jnp.sin(angles)
    query_heads = query_plain.reshape(tok_rows, head_count, NOPE)
    query_rot = rotate(
        query_turn.reshape(tok_rows, head_count, ROPE).astype(jnp.float32),
        cosine[:, None, :],
        sine[:, None, :],
    ).astype(jnp.bfloat16)
    latent = rms_scale(latent_raw.astype(jnp.float32), latent_gain).astype(jnp.bfloat16)
    key_rot = rotate(shared_key.astype(jnp.float32), cosine, sine).astype(jnp.bfloat16)
    softmax_scale = (NOPE + ROPE) ** (-0.5)

    def attend_block(state, key_plain, values, key_pos):
        run_max, run_total, run_acc = state
        score = jnp.einsum(
            "qhd,khd->hqk", query_heads, key_plain, preferred_element_type=jnp.float32
        )
        score = score + jnp.einsum(
            "qhr,kr->hqk", query_rot, key_pos, preferred_element_type=jnp.float32
        )
        score = score * softmax_scale
        new_max = jnp.maximum(run_max, jnp.max(score, axis=-1))
        shrink = jnp.exp(run_max - new_max)
        expo = jnp.exp(score - new_max[:, :, None])
        run_total = run_total * shrink + jnp.sum(expo, axis=-1)
        run_acc = run_acc * shrink.T[:, :, None] + jnp.einsum(
            "hqk,khd->qhd", expo.astype(jnp.bfloat16), values, preferred_element_type=jnp.float32
        )
        return (new_max, run_total, run_acc)

    start_state = (
        jnp.full((head_count, tok_rows), -jnp.inf, jnp.float32),
        jnp.zeros((head_count, tok_rows), jnp.float32),
        jnp.zeros((tok_rows, head_count, V), jnp.float32),
    )
    state = start_state
    latent_piece = lax.all_gather(latent, "sp", axis=0, tiled=True)
    pos_piece = lax.all_gather(key_rot, "sp", axis=0, tiled=True)
    piece_len = latent_piece.shape[0]
    block_len = math.gcd(piece_len, 512)
    block_count = piece_len // block_len

    def one_block(inner, items):
        latent_rows, pos_rows = items
        key_plain = (
            jnp.dot(latent_rows, key_up, preferred_element_type=jnp.float32)
            .astype(jnp.bfloat16)
            .reshape(block_len, head_count, NOPE)
        )
        values = (
            jnp.dot(latent_rows, value_up, preferred_element_type=jnp.float32)
            .astype(jnp.bfloat16)
            .reshape(block_len, head_count, V)
        )
        return (attend_block(inner, key_plain, values, pos_rows), None)

    state, unused = lax.scan(
        one_block,
        state,
        (
            latent_piece.reshape(block_count, block_len, latent_piece.shape[1]),
            pos_piece.reshape(block_count, block_len, ROPE),
        ),
    )
    attended = (
        (state[2] / state[1].T[:, :, None]).astype(jnp.bfloat16).reshape(tok_rows, head_count * V)
    )
    own_start = lax.axis_index("tp") * part_rows
    mixed = lax.psum_scatter(
        jnp.dot(attended, out_weight, preferred_element_type=jnp.float32).astype(jnp.bfloat16),
        "tp",
        scatter_dimension=0,
        tiled=True,
    ).astype(jnp.float32)
    middle = lax.dynamic_slice_in_dim(resid_in, own_start, part_rows, 0).astype(jnp.float32) + mixed
    normed = rms_scale(middle, mixer_gain).astype(jnp.bfloat16)
    all_rows = lax.all_gather(normed, "tp", axis=0, tiled=True)
    gate_sum = jnp.dot(
        all_rows,
        lax.all_gather(gate_weight, "sp", axis=0, tiled=True),
        preferred_element_type=jnp.float32,
    )
    up_sum = jnp.dot(
        all_rows,
        lax.all_gather(up_weight, "sp", axis=0, tiled=True),
        preferred_element_type=jnp.float32,
    )
    hidden = (jax.nn.silu(gate_sum) * up_sum).astype(jnp.bfloat16)
    terms = jnp.dot(
        hidden,
        lax.all_gather(down_weight, "sp", axis=1, tiled=True),
        preferred_element_type=jnp.float32,
    )
    down_sum = lax.psum_scatter(
        terms.astype(jnp.bfloat16), "tp", scatter_dimension=0, tiled=True
    ).astype(jnp.float32)
    return (middle + 0.5 * down_sum).astype(jnp.bfloat16)

MESH = pl.DeviceIdType.MESH
BF = jnp.bfloat16
F32 = jnp.float32
BY_LAST = (((1,), (1,)), ((), ()))


def turn(values, cosine, sine):
    width = values.shape[-1]
    half = ROPE // 2
    lane = lax.broadcasted_iota(jnp.int32, values.shape, 1) % ROPE
    swapped = jnp.where(lane < half, pltpu.roll(values, width - half, 1), pltpu.roll(values, half, 1))
    return values * cosine + swapped * sine


def layer_kernel(
    sizes,
    latent_ref,
    shared_ref,
    inv_ref,
    lgain_ref,
    mgain_ref,
    query_hbm,
    turn_hbm,
    kup_hbm,
    vup_hbm,
    ow_hbm,
    resid_hbm,
    gate_hbm,
    up_hbm,
    down_hbm,
    out_ref,
    query_ref,
    turn_ref,
    kup_ref,
    vup_ref,
    ow_ref,
    resid_ref,
    raw_buf,
    wt_buf,
    kv_buf,
    key_buf,
    val_buf,
    att_buf,
    mix_buf,
    mixb_buf,
    mixr_buf,
    mid_buf,
    w_buf,
    wd_buf,
    n_buf,
    h_buf,
    acc_buf,
    r_buf,
    load_sem,
    l_ssem,
    l_rsem,
    f_ssem,
    f_rsem,
    m_ssem,
    m_rsem,
    w_ssem,
    w_rsem,
    x_ssem,
    x_rsem,
    a_ssem,
    a_rsem,
    s_ssem,
    s_rsem,
):
    sp, tp = sizes
    s = lax.axis_index("sp")
    t = lax.axis_index("tp")
    core = t % 2
    x = t // 2
    y = s % 2
    zl = (s // 2) % 2
    zh = s // 4
    other = t + 1 - 2 * core
    rows = latent_ref.shape[0]
    half_rows = rows // 2
    part = rows // tp
    hid, cols = down_hbm.shape[1:]
    kv_width = latent_ref.shape[1]
    lanes = cols // 2

    def ring(q):
        flip = lambda bit, by: bit + by * (1 - 2 * bit)
        return flip(zh, q // 4) * 4 + flip(zl, q // 2 % 2) * 2 + flip(y, q % 2)

    def remote(src, dst, ssem, rsem, dev):
        return pltpu.make_async_remote_copy(
            src_ref=src, dst_ref=dst, send_sem=ssem, recv_sem=rsem, device_id=dev, device_id_type=MESH
        )

    sends = []

    def send(src, dst, ssem, rsem, dev):
        cp = remote(src, dst, ssem, rsem, dev)
        cp.start()
        sends.append(cp)

    def arrived(ref, rsem):
        remote(ref, ref, rsem, rsem, (s, other)).wait_recv()

    barrier = pltpu.get_barrier_semaphore()
    for q in range(1, sp):
        pl.semaphore_signal(barrier, inc=1, device_id=(ring(q), t), device_id_type=MESH)
    for j in range(1, tp):
        pl.semaphore_signal(barrier, inc=1, device_id=(s, (t + j) % tp), device_id_type=MESH)

    own_rows = pl.ds(pl.multiple_of(t * part, part), part)
    own_cols = pl.ds(pl.multiple_of(s * cols, cols), cols)
    own_lanes = pl.ds(pl.multiple_of(s * lanes, lanes), lanes)
    loads = [
        pltpu.make_async_copy(src, dst, load_sem.at[i])
        for i, (src, dst) in enumerate(
            [
                (gate_hbm, raw_buf.at[0]),
                (up_hbm, raw_buf.at[1]),
                (kup_hbm, kup_ref),
                (vup_hbm, vup_ref),
                (turn_hbm, turn_ref),
                (query_hbm, query_ref),
                (ow_hbm, ow_ref),
                (resid_hbm.at[own_rows], resid_ref),
                (down_hbm.at[s, :, :lanes], wd_buf.at[0, core, :, own_lanes]),
                (down_hbm.at[s, :, lanes:], wd_buf.at[1, core, :, own_lanes]),
            ]
        )
    ]
    for load in loads:
        load.start()

    position = (s * rows + lax.broadcasted_iota(jnp.int32, (rows, 128), 0)).astype(F32)
    angles = position * inv_ref[...]
    sign = jnp.where(lax.broadcasted_iota(jnp.int32, (rows, 128), 1) % ROPE < ROPE // 2, -1.0, 1.0)
    cosine = jnp.cos(angles)
    sine = jnp.sin(angles) * sign
    lat = latent_ref[...].astype(F32)
    lat = lat * lax.rsqrt(jnp.mean(lat * lat, axis=-1, keepdims=True) + 1e-06) * lgain_ref[...]
    own_lat = lat.astype(BF)
    shared = shared_ref[...].astype(F32)
    shared = jnp.concatenate([shared] * (128 // ROPE), axis=0).T
    own_key = turn(shared, cosine, sine).astype(BF)
    for half in range(2):
        part_of = slice(half * half_rows, (half + 1) * half_rows)
        kv_buf[0, half, :, :kv_width] = own_lat[part_of]
        kv_buf[0, half, :, kv_width:] = own_key[part_of]

    pl.semaphore_wait(barrier, sp - 1 + tp - 1)

    def send_latent(slot, by):
        to = slot + by
        send(kv_buf.at[slot, core], kv_buf.at[to, core], l_ssem.at[to], l_rsem.at[to], (ring(by), t))

    for by in (4, 6, 2, 1):
        send_latent(0, by)

    for which in range(2):
        loads[which].wait()
        for j in range(raw_buf.shape[2] // 128):
            tile = slice(j * 128, (j + 1) * 128)
            wt_buf[which, tile, :] = raw_buf[which, :, tile].T

    def hid_rows(dest):
        return pl.ds(pl.multiple_of(dest * hid, 16), hid)

    def weight_slot(which, lane_of, side=core):
        if which < 2:
            return w_buf.at[which, side, :, pl.ds(pl.multiple_of(lane_of * cols, cols), cols)]
        return wd_buf.at[which - 2, side, :, pl.ds(pl.multiple_of(lane_of * lanes, lanes), lanes)]

    def send_weights(some):
        for which, q in some:
            dest = ring(q)
            if which < 2:
                src = wt_buf.at[which, hid_rows(dest), :]
            else:
                src = down_hbm.at[dest, :, (which - 2) * lanes:(which - 1) * lanes]
            send(src, weight_slot(which, s), w_ssem.at[which, q], w_rsem.at[which, q], (dest, t))

    def pass_weights(some):
        for which, q in some:
            slot = weight_slot(which, ring(q))
            if q:
                arrived(slot, w_rsem.at[which, q])
            send(slot, slot, x_ssem.at[which, q], x_rsem.at[which, q], (s, other))

    def passed_weights(which):
        for q in range(sp):
            arrived(weight_slot(which, ring(q), 1 - core), x_rsem.at[which, q])

    near = [(w, q) for q in (1, 3, 2) for w in range(2)]
    far = [(w, q) for q in (7, 5, 6, 4) for w in range(2)]
    first = far[:2] + near[:2] + far[2:3] + near[2:3] + far[3:4] + near[3:4] + far[4:5]
    second = far[5:6]
    third = far[6:7] + near[4:5] + far[7:] + near[5:]
    fourth = [(w, q) for w in (2, 3) for q in (7, 5, 6, 4, 3, 2, 1)]

    send_weights(first)
    for which in range(2):
        w_buf[which, core, :, own_cols] = wt_buf[which, hid_rows(s), :]

    def make_kv(k):
        piece = kv_buf[k].reshape(rows, kv_buf.shape[3])
        piece_lat = piece[:, :kv_width]
        key_buf[k * rows:(k + 1) * rows, :] = jnp.dot(
            piece_lat, kup_ref[...], preferred_element_type=F32
        ).astype(BF)
        val_buf[k * rows:(k + 1) * rows, :] = jnp.dot(
            piece_lat, vup_ref[...], preferred_element_type=F32
        ).astype(BF)

    for load in loads[2:]:
        load.wait()
    make_kv(0)
    query_rot = turn(
        turn_ref[...].astype(F32),
        jnp.concatenate([cosine] * (turn_ref.shape[1] // 128), axis=1),
        jnp.concatenate([sine] * (turn_ref.shape[1] // 128), axis=1),
    ).astype(BF)

    def pass_latent(slot):
        send(kv_buf.at[slot, core], kv_buf.at[slot, core], f_ssem.at[slot], f_rsem.at[slot], (s, other))

    for slot in (2, 4, 6, 1, 3, 5, 7):
        arrived(kv_buf.at[slot, core], l_rsem.at[slot])
        if slot % 2 == 0:
            send_latent(slot, 1)
        pass_latent(slot)
    for slot in (2, 4, 6, 1, 3, 5, 7):
        arrived(kv_buf.at[slot, 1 - core], f_rsem.at[slot])
        make_kv(slot)

    scale = (NOPE + ROPE) ** (-0.5)
    all_rot = kv_buf[...].reshape(sp * rows, kv_buf.shape[3])[:, kv_width:]
    lane = lax.broadcasted_iota(jnp.int32, (rows, 128), 1)
    for pair in range(query_ref.shape[1] // 128):
        span = slice(pair * 128, (pair + 1) * 128)
        keys = jnp.concatenate([key_buf[:, span], all_rot], axis=1)
        vals = val_buf[:, span]
        results = []
        for inner in range(2):
            head = pair * 2 + inner
            tile = head * ROPE // 128
            group = head % (128 // ROPE)
            q_plain = jnp.where(lane // NOPE == inner, query_ref[:, span], jnp.zeros((), BF))
            q_turn = jnp.where(
                lane // ROPE == group, query_rot[:, tile * 128:(tile + 1) * 128], jnp.zeros((), BF)
            )
            score = lax.dot_general(
                jnp.concatenate([q_plain, q_turn], axis=1), keys, BY_LAST, preferred_element_type=F32
            ) * scale
            top = jnp.max(score, axis=-1, keepdims=True)
            expo = jnp.exp(score - top)
            total = jnp.sum(expo, axis=-1, keepdims=True)
            results.append(jnp.dot(expo.astype(BF), vals, preferred_element_type=F32) / total)
        att_buf[:, span] = jnp.where(lane < V, results[0], results[1]).astype(BF)

    mix_buf[...] = jnp.dot(att_buf[...], ow_ref[...], preferred_element_type=F32)
    mixb_buf[...] = mix_buf[...].astype(BF).reshape(mixb_buf.shape)
    for j in range(1, tp):
        dest = (t + j) % tp
        send(mixb_buf.at[dest], mixr_buf.at[j], m_ssem.at[j], m_rsem.at[j], (s, dest))
    mid = resid_ref[...].astype(F32) + mix_buf[own_rows, :]
    for j in range(1, tp):
        arrived(mixr_buf.at[j], m_rsem.at[j])
        mid = mid + mixr_buf[j].astype(F32)
    mid_buf[...] = mid
    normed = mid * lax.rsqrt(jnp.mean(mid * mid, axis=-1, keepdims=True) + 1e-06) * mgain_ref[...]
    n_buf[0] = normed.astype(BF)

    a_x = 1 - core
    along_x = ((s, (1 - x) * 2 + core))
    along_y = (ring(1), t)
    pick = lambda first_x, i: first_x * along_x[i] + (1 - first_x) * along_y[i]
    steps = (
        (8, (pick(a_x, 0), pick(a_x, 1))),
        (4, (pick(core, 0), pick(core, 1))),
        (2, (ring(2), t)),
        (1, (ring(4), t)),
    )

    def spread(slot):
        for by, dev in reversed(steps):
            if by > slot:
                to = slot + by
                send(n_buf.at[slot], n_buf.at[to], a_ssem.at[to], a_rsem.at[to], dev)

    spread(0)
    send_weights(second)
    arrived(n_buf.at[1], a_rsem.at[1])
    spread(1)
    send_weights(third)
    for slot in (2, 3):
        arrived(n_buf.at[slot], a_rsem.at[slot])
        spread(slot)
    send_weights(fourth)
    for slot in (4, 5, 6, 7):
        arrived(n_buf.at[slot], a_rsem.at[slot])
        spread(slot)
    pass_weights([(w, 0) for w in range(2)] + first + second + third)
    for slot in range(8, 16):
        arrived(n_buf.at[slot], a_rsem.at[slot])
    passed_weights(0)
    passed_weights(1)

    group = n_buf.shape[0] // 2
    gate_w = w_buf[0].reshape(2 * hid, w_buf.shape[3])
    up_w = w_buf[1].reshape(2 * hid, w_buf.shape[3])
    for g in range(2):
        block = n_buf[g * group:(g + 1) * group].reshape(group * part, n_buf.shape[2])
        gate = lax.dot_general(block, gate_w, BY_LAST, preferred_element_type=F32)
        up = lax.dot_general(block, up_w, BY_LAST, preferred_element_type=F32)
        h_buf[g * group * part:(g + 1) * group * part, :] = (gate / (1.0 + jnp.exp(-gate)) * up).astype(BF)

    def sums(h, slot, count):
        by, dev = next(step for step in steps if slot >= step[0])
        some = pl.ds(slot, count)
        send(acc_buf.at[h, some], r_buf.at[h, some], s_ssem.at[h, slot], s_rsem.at[h, slot], dev)

    def project(h):
        weights = wd_buf[h].reshape(2 * hid, wd_buf.shape[3])
        for g in (1, 0):
            down = jnp.dot(
                h_buf[g * group * part:(g + 1) * group * part, :], weights, preferred_element_type=F32
            )
            acc_buf[h, g * group:(g + 1) * group] = down.astype(BF).reshape(
                group, part, acc_buf.shape[3]
            )
            if g:
                for slot in (14, 12, 10, 8):
                    sums(h, slot, 2)

    def join(h, slot, count, by):
        some = slice(slot + by, slot + by + count)
        arrived(r_buf.at[h, pl.ds(slot + by, count)], s_rsem.at[h, slot + by])
        acc_buf[h, slot:slot + count] = (
            acc_buf[h, slot:slot + count].astype(F32) + r_buf[h, some].astype(F32)
        ).astype(BF)

    def reduce_first(h):
        for slot in (6, 4):
            join(h, slot, 2, 8)
            sums(h, slot, 2)

    def reduce_second(h):
        join(h, 2, 2, 8)
        join(h, 2, 2, 4)
        sums(h, 2, 2)

    def reduce_third(h):
        join(h, 0, 2, 8)
        join(h, 0, 2, 4)
        join(h, 0, 2, 2)
        sums(h, 1, 1)

    def finish(h):
        arrived(r_buf.at[h, pl.ds(1, 1)], s_rsem.at[h, 1])
        value = acc_buf[h, 0].astype(F32) + r_buf[h, 1].astype(F32)
        for k in range(sp):
            span = slice(k * cols + h * lanes, k * cols + (h + 1) * lanes)
            out_ref[:, span] = (
                mid_buf[:, span] + 0.5 * value[:, k * lanes:(k + 1) * lanes]
            ).astype(BF)

    down_part = [[(w, q) for q in range(sp)] for w in (2, 3)]
    pass_weights(down_part[0])
    passed_weights(2)
    project(0)
    reduce_first(0)
    pass_weights(down_part[1])
    reduce_second(0)
    passed_weights(3)
    project(1)
    reduce_third(0)
    reduce_first(1)
    reduce_second(1)
    finish(0)
    reduce_third(1)
    finish(1)

    for cp in sends:
        cp.wait_send()


def fused_layer(
    resid_in,
    query_plain,
    query_turn,
    latent_raw,
    shared_key,
    latent_gain,
    key_up,
    value_up,
    out_weight,
    mixer_gain,
    gate_weight,
    up_weight,
    down_weight,
):
    sp = lax.axis_size("sp")
    tp = lax.axis_size("tp")
    rows, width = resid_in.shape
    part = rows // tp
    hid = down_weight.shape[0] // sp
    cols = down_weight.shape[1]
    kv = latent_raw.shape[1]
    heads_width = query_plain.shape[1]
    inverse = 10000.0 ** (-jnp.arange(0, ROPE, 2, dtype=F32) / ROPE)
    inverse_lanes = jnp.tile(inverse, 128 * 2 // ROPE)[None, :]
    chips = sp * tp // 2
    dma = pltpu.SemaphoreType.DMA
    vmem = lambda *shape: pltpu.VMEM(shape, BF)
    near = pl.BlockSpec(memory_space=pltpu.VMEM)
    far = pl.BlockSpec(memory_space=pl.ANY)
    return pl.pallas_call(
        functools.partial(layer_kernel, (sp, tp)),
        out_shape=jax.ShapeDtypeStruct((part, width), BF),
        in_specs=[near] * 5 + [far] * 9,
        out_specs=near,
        scratch_shapes=[
            vmem(*query_plain.shape),
            vmem(*query_turn.shape),
            vmem(*key_up.shape),
            vmem(*value_up.shape),
            vmem(*out_weight.shape),
            vmem(part, width),
            vmem(2, *gate_weight.shape),
            vmem(2, *gate_weight.shape[::-1]),
            vmem(sp, 2, rows // 2, kv + 128),
            vmem(sp * rows, heads_width),
            vmem(sp * rows, heads_width),
            vmem(rows, heads_width),
            pltpu.VMEM((rows, width), F32),
            vmem(tp, part, width),
            vmem(tp, part, width),
            pltpu.VMEM((part, width), F32),
            vmem(2, 2, hid, width),
            vmem(2, 2, hid, width // 2),
            vmem(chips, part, width),
            vmem(chips * part, 2 * hid),
            vmem(2, chips, part, width // 2),
            vmem(2, chips, part, width // 2),
            dma((10,)),
            dma((sp,)),
            dma((sp,)),
            dma((sp,)),
            dma((sp,)),
            dma((tp,)),
            dma((tp,)),
            dma((4, sp)),
            dma((4, sp)),
            dma((4, sp)),
            dma((4, sp)),
            dma((chips,)),
            dma((chips,)),
            dma((2, chips)),
            dma((2, chips)),
        ],
        compiler_params=pltpu.CompilerParams(
            collective_id=0, has_side_effects=True, vmem_limit_bytes=60 * 1024 * 1024
        ),
    )(
        latent_raw,
        shared_key.T,
        inverse_lanes,
        latent_gain[None, :],
        mixer_gain[None, :],
        query_plain,
        query_turn,
        key_up,
        value_up,
        out_weight,
        resid_in,
        gate_weight,
        up_weight,
        down_weight.reshape(sp, hid, cols),
    )


def per_device(*arrays):
    resid_in, query_plain, query_turn, latent_raw = arrays[:4]
    down_weight = arrays[-1]
    sp = lax.axis_size("sp")
    tp = lax.axis_size("tp")
    rows = resid_in.shape[0]
    fits = (
        sp // 4 == 2
        and tp // 2 == 2
        and rows % (32 * tp) == 0
        and down_weight.shape[0] % (16 * sp) == 0
        and down_weight.shape[1] % 128 == 0
        and latent_raw.shape[1] % 128 == 0
        and query_plain.shape[1] % 128 == 0
        and query_turn.shape[1] % 128 == 0
        and rows * sp <= 1024
        and sp * tp <= 32
    )
    if fits:
        return fused_layer(*arrays)
    return plain_layer(*arrays)


def solution(mesh):
    return jax.shard_map(
        per_device,
        mesh=mesh,
        in_specs=(
            P("sp", None),
            P("sp", "tp"),
            P("sp", "tp"),
            P("sp", None),
            P("sp", None),
            P(),
            P(None, "tp"),
            P(None, "tp"),
            P("tp", None),
            P(),
            P("sp", "tp"),
            P("sp", "tp"),
            P("tp", "sp"),
        ),
        out_specs=P(("sp", "tp"), None),
        check_vma=False,
    )
```

time: 127 us -> 107 us (0.84)
  Pallas kernels: 119 us -> 104 us
  local copies, waits for them, and re-layouts: 6.52 us -> 2.17 us
    pallas_call x1, Pallas kernels: 119 us -> 104 us  [fused_layer(): pl.pallas_call(functools.partial(layer_kernel, (sp, tp)), out_shape=jax.S...]
    transpose x2 -> x0, local copies, waits for them, and re-layouts: 3.39 us -> none  [the longest x1 2.24 us: fused_layer(): gate_weight.T.reshape(sp, hid, cols)]
where the time goes in v1:
time: 107 us
  Pallas kernels  104 us (97%)
  local copies, waits for them, and re-layouts  2.17 us (2%)
    pallas_call x1, Pallas kernels, fused_layer(): pl.pallas_call(functools.partial(layer_kernel, (sp, tp)), out_shape=jax.S...  104 us

profile of v1, /device:TPU:0, one launch (start us, length us, event | category | flops | bytes accessed | tf_op | source)
XLA Modules:
  0.0 106.7 jit_solution(14012989995319339452)
XLA Ops:
  0.0 0.6 broadcast_in_dim_tile.3.inv_ref
  0.6 104.5 %shard_map.127 = bf16[32,2048]{1,0:T(8,128)(2,1)} custom-call(bf16[128,256]{1,0:T(8,128)(2,1)} %latent_ref.1, bf16[32,128]{1,0:T(8,128)(2,1)} %bitcast.5, f32[1,128]{1,0:T(1,128)} %broadcast_in_dim_tile.3.inv_ref, f32[1,256]{1,0:T(1,128)} %bitcast.7, f32[1,2048]{1,0:T(1,128)} %bitcast.6, bf16[128,512]{1,0:T(8,128)(2,1)} %query_hbm.1, ...), custom_call_target="tpu_custom_call" | custom-call | tf_op jit(solution)/shard_map/pallas_call | solution.py:565
  105.1 1.6 %copy.15 = bf16[32,2048]{1,0:T(8,128)(2,1)} copy(bf16[32,2048]{1,0:T(8,128)(2,1)} %shard_map.127) | data formatting | bytes 262144
  (2 shorter events, 0.0 us)

commit v2 on v1

--- a/solution.py
+++ b/solution.py
@@ -185,13 +185,16 @@
     resid_ref,
     raw_buf,
     wt_buf,
+    relay_buf,
     kv_buf,
     key_buf,
     val_buf,
     att_buf,
     mix_buf,
-    mixb_buf,
-    mixr_buf,
+    pair_buf,
+    paird_buf,
+    cross_buf,
+    crossr_buf,
     mid_buf,
     w_buf,
     wd_buf,
@@ -208,6 +211,8 @@
     m_rsem,
     w_ssem,
     w_rsem,
+    y_ssem,
+    y_rsem,
     x_ssem,
     x_rsem,
     a_ssem,
@@ -230,6 +235,8 @@
     hid, cols = down_hbm.shape[1:]
     kv_width = latent_ref.shape[1]
     lanes = cols // 2
+    width = ow_hbm.shape[1]
+    along_x = (s, (1 - x) * 2 + core)
 
     def ring(q):
         flip = lambda bit, by: bit + by * (1 - 2 * bit)
@@ -240,12 +247,11 @@
             src_ref=src, dst_ref=dst, send_sem=ssem, recv_sem=rsem, device_id=dev, device_id_type=MESH
         )
 
-    sends = []
-
     def send(src, dst, ssem, rsem, dev):
-        cp = remote(src, dst, ssem, rsem, dev)
-        cp.start()
-        sends.append(cp)
+        remote(src, dst, ssem, rsem, dev).start()
+
+    def sent(ref, ssem):
+        remote(ref, ref, ssem, ssem, (s, other)).wait_send()
 
     def arrived(ref, rsem):
         remote(ref, ref, rsem, rsem, (s, other)).wait_recv()
@@ -273,6 +279,7 @@
                 (resid_hbm.at[own_rows], resid_ref),
                 (down_hbm.at[s, :, :lanes], wd_buf.at[0, core, :, own_lanes]),
                 (down_hbm.at[s, :, lanes:], wd_buf.at[1, core, :, own_lanes]),
+                (down_hbm, wt_buf.at[2]),
             ]
         )
     ]
@@ -297,57 +304,82 @@
 
     pl.semaphore_wait(barrier, sp - 1 + tp - 1)
 
+    along_y = (ring(1), t)
+
     def send_latent(slot, by):
         to = slot + by
-        send(kv_buf.at[slot, core], kv_buf.at[to, core], l_ssem.at[to], l_rsem.at[to], (ring(by), t))
-
-    for by in (4, 6, 2, 1):
+        send(kv_buf.at[slot, core], kv_buf.at[to, core], l_ssem.at[0], l_rsem.at[to], (ring(by), t))
+
+    for by in (6, 4, 2, 1):
         send_latent(0, by)
 
     for which in range(2):
         loads[which].wait()
+        turned_buf = wt_buf.at[which].reshape(sp * hid, cols)
         for j in range(raw_buf.shape[2] // 128):
             tile = slice(j * 128, (j + 1) * 128)
-            wt_buf[which, tile, :] = raw_buf[which, :, tile].T
-
-    def hid_rows(dest):
-        return pl.ds(pl.multiple_of(dest * hid, 16), hid)
+            turned_buf[tile, :] = raw_buf[which, :, tile].T
+
+    first = [(0, 6), (1, 6), (0, 4), (1, 4)]
+    second = [(0, 7)]
+    third = [(1, 7), (0, 5), (1, 5), (0, 2), (1, 2), (0, 3), (1, 3)]
+    fourth = [(w, q) for w in (2, 3) for q in (6, 7, 4, 5, 2, 3)]
+
+    def late(which, q):
+        return int((which, q) not in first and (q != 1 or which > 1))
 
     def weight_slot(which, lane_of, side=core):
         if which < 2:
             return w_buf.at[which, side, :, pl.ds(pl.multiple_of(lane_of * cols, cols), cols)]
         return wd_buf.at[which - 2, side, :, pl.ds(pl.multiple_of(lane_of * lanes, lanes), lanes)]
 
+    def lanes_of(ref, which):
+        return ref if which < 2 else ref.at[:, (which - 2) * lanes:(which - 1) * lanes]
+
     def send_weights(some):
         for which, q in some:
-            dest = ring(q)
-            if which < 2:
-                src = wt_buf.at[which, hid_rows(dest), :]
+            kind = min(which, 2)
+            if q > 1 and q % 2:
+                src, owner, dest = relay_buf.at[kind, q // 2 - 1], ring(1), (ring(q - 1), t)
             else:
-                src = down_hbm.at[dest, :, (which - 2) * lanes:(which - 1) * lanes]
-            send(src, weight_slot(which, s), w_ssem.at[which, q], w_rsem.at[which, q], (dest, t))
-
-    def pass_weights(some):
-        for which, q in some:
+                src, owner, dest = wt_buf.at[kind, ring(q)], s, (ring(q), t)
+            send(
+                lanes_of(src, which),
+                weight_slot(which, owner),
+                w_ssem.at[which],
+                w_rsem.at[which, late(which, q)],
+                dest,
+            )
+
+    def send_relays(kind):
+        for q in (7, 5, 3):
+            send(
+                wt_buf.at[kind, ring(q)], relay_buf.at[kind, q // 2 - 1], y_ssem.at[kind], y_rsem.at[kind], along_y
+            )
+        send_weights([(which, 1) for which in ((kind,) if kind < 2 else (2, 3))])
+
+    def relayed(kind):
+        arrived(relay_buf.at[kind], y_rsem.at[kind])
+
+    def some_of(which, side, count):
+        if which < 2:
+            return w_buf.at[which, side, :, :count * cols]
+        return wd_buf.at[which - 2, side, :, :count * lanes]
+
+    def pass_weights(which, group):
+        some = [q for q in range(1, sp) if late(which, q) == group]
+        arrived(some_of(which, core, len(some)), w_rsem.at[which, group])
+        for q in some + [0] * group:
             slot = weight_slot(which, ring(q))
-            if q:
-                arrived(slot, w_rsem.at[which, q])
-            send(slot, slot, x_ssem.at[which, q], x_rsem.at[which, q], (s, other))
+            send(slot, slot, x_ssem.at[which], x_rsem.at[which], (s, other))
 
     def passed_weights(which):
-        for q in range(sp):
-            arrived(weight_slot(which, ring(q), 1 - core), x_rsem.at[which, q])
-
-    near = [(w, q) for q in (1, 3, 2) for w in range(2)]
-    far = [(w, q) for q in (7, 5, 6, 4) for w in range(2)]
-    first = far[:2] + near[:2] + far[2:3] + near[2:3] + far[3:4] + near[3:4] + far[4:5]
-    second = far[5:6]
-    third = far[6:7] + near[4:5] + far[7:] + near[5:]
-    fourth = [(w, q) for w in (2, 3) for q in (7, 5, 6, 4, 3, 2, 1)]
-
-    send_weights(first)
+        arrived(some_of(which, 1 - core, sp), x_rsem.at[which])
+
+    send_relays(0)
+    send_relays(1)
     for which in range(2):
-        w_buf[which, core, :, own_cols] = wt_buf[which, hid_rows(s), :]
+        w_buf[which, core, :, own_cols] = wt_buf[which, s]
 
     def make_kv(k):
         piece = kv_buf[k].reshape(rows, kv_buf.shape[3])
@@ -359,7 +391,7 @@
             piece_lat, vup_ref[...], preferred_element_type=F32
         ).astype(BF)
 
-    for load in loads[2:]:
+    for load in loads[2:10]:
         load.wait()
     make_kv(0)
     query_rot = turn(
@@ -369,14 +401,22 @@
     ).astype(BF)
 
     def pass_latent(slot):
-        send(kv_buf.at[slot, core], kv_buf.at[slot, core], f_ssem.at[slot], f_rsem.at[slot], (s, other))
-
-    for slot in (2, 4, 6, 1, 3, 5, 7):
+        send(kv_buf.at[slot, core], kv_buf.at[slot, core], f_ssem.at[0], f_rsem.at[slot], (s, other))
+
+    def take_latent(slot):
         arrived(kv_buf.at[slot, core], l_rsem.at[slot])
-        if slot % 2 == 0:
-            send_latent(slot, 1)
         pass_latent(slot)
-    for slot in (2, 4, 6, 1, 3, 5, 7):
+
+    take_latent(1)
+    for by in (6, 4, 2):
+        send_latent(1, by)
+    loads[10].wait()
+    send_relays(2)
+    order = (2, 4, 6, 3, 5, 7)
+    for slot in order:
+        take_latent(slot)
+    send_weights(first)
+    for slot in (1,) + order:
         arrived(kv_buf.at[slot, 1 - core], f_rsem.at[slot])
         make_kv(slot)
 
@@ -405,22 +445,31 @@
             results.append(jnp.dot(expo.astype(BF), vals, preferred_element_type=F32) / total)
         att_buf[:, span] = jnp.where(lane < V, results[0], results[1]).astype(BF)
 
-    mix_buf[...] = jnp.dot(att_buf[...], ow_ref[...], preferred_element_type=F32)
-    mixb_buf[...] = mix_buf[...].astype(BF).reshape(mixb_buf.shape)
-    for j in range(1, tp):
-        dest = (t + j) % tp
-        send(mixb_buf.at[dest], mixr_buf.at[j], m_ssem.at[j], m_rsem.at[j], (s, dest))
-    mid = resid_ref[...].astype(F32) + mix_buf[own_rows, :]
-    for j in range(1, tp):
-        arrived(mixr_buf.at[j], m_rsem.at[j])
-        mid = mid + mixr_buf[j].astype(F32)
+    span_of = [slice(c * width // 2, (c + 1) * width // 2) for c in range(2)]
+    for c, span in enumerate(span_of):
+        mix = jnp.dot(att_buf[...], ow_ref[:, span], preferred_element_type=F32)
+        mix_buf[:, span] = mix
+        for dest in range(tp):
+            pair_buf[dest % 2, c, dest // 2] = mix[dest * part:(dest + 1) * part].astype(BF)
+        send(pair_buf.at[1 - core, c], paird_buf.at[c], m_ssem.at[c], m_rsem.at[c], (s, other))
+    cross_rows = pl.ds(pl.multiple_of(((1 - x) * 2 + core) * part, part), part)
+    for c, span in enumerate(span_of):
+        arrived(paird_buf.at[c], m_rsem.at[c])
+        cross_buf[c] = (mix_buf[cross_rows, span] + paird_buf[c, 1 - x].astype(F32)).astype(BF)
+        send(cross_buf.at[c], crossr_buf.at[c], m_ssem.at[2 + c], m_rsem.at[2 + c], along_x)
+    mids = [
+        resid_ref[:, span].astype(F32) + mix_buf[own_rows, span] + paird_buf[c, x].astype(F32)
+        for c, span in enumerate(span_of)
+    ]
+    for c in range(2):
+        arrived(crossr_buf.at[c], m_rsem.at[2 + c])
+        mids[c] = mids[c] + crossr_buf[c].astype(F32)
+    mid = jnp.concatenate(mids, axis=1)
     mid_buf[...] = mid
     normed = mid * lax.rsqrt(jnp.mean(mid * mid, axis=-1, keepdims=True) + 1e-06) * mgain_ref[...]
     n_buf[0] = normed.astype(BF)
 
     a_x = 1 - core
-    along_x = ((s, (1 - x) * 2 + core))
-    along_y = (ring(1), t)
     pick = lambda first_x, i: first_x * along_x[i] + (1 - first_x) * along_y[i]
     steps = (
         (8, (pick(a_x, 0), pick(a_x, 1))),
@@ -433,23 +482,27 @@
         for by, dev in reversed(steps):
             if by > slot:
                 to = slot + by
-                send(n_buf.at[slot], n_buf.at[to], a_ssem.at[to], a_rsem.at[to], dev)
+                send(n_buf.at[slot], n_buf.at[to], a_ssem.at[0], a_rsem.at[min(to, sp)], dev)
 
     spread(0)
+    relayed(0)
     send_weights(second)
     arrived(n_buf.at[1], a_rsem.at[1])
     spread(1)
+    relayed(1)
     send_weights(third)
     for slot in (2, 3):
         arrived(n_buf.at[slot], a_rsem.at[slot])
         spread(slot)
+    relayed(2)
     send_weights(fourth)
+    pass_weights(0, 0)
+    pass_weights(1, 0)
     for slot in (4, 5, 6, 7):
         arrived(n_buf.at[slot], a_rsem.at[slot])
         spread(slot)
-    pass_weights([(w, 0) for w in range(2)] + first + second + third)
-    for slot in range(8, 16):
-        arrived(n_buf.at[slot], a_rsem.at[slot])
+    pass_weights(0, 1)
+    pass_weights(1, 1)
     passed_weights(0)
     passed_weights(1)
 
@@ -457,6 +510,8 @@
     gate_w = w_buf[0].reshape(2 * hid, w_buf.shape[3])
     up_w = w_buf[1].reshape(2 * hid, w_buf.shape[3])
     for g in range(2):
+        if g:
+            arrived(n_buf.at[pl.ds(group, group)], a_rsem.at[sp])
         block = n_buf[g * group:(g + 1) * group].reshape(group * part, n_buf.shape[2])
         gate = lax.dot_general(block, gate_w, BY_LAST, preferred_element_type=F32)
         up = lax.dot_general(block, up_w, BY_LAST, preferred_element_type=F32)
@@ -465,7 +520,7 @@
     def sums(h, slot, count):
         by, dev = next(step for step in steps if slot >= step[0])
         some = pl.ds(slot, count)
-        send(acc_buf.at[h, some], r_buf.at[h, some], s_ssem.at[h, slot], s_rsem.at[h, slot], dev)
+        send(acc_buf.at[h, some], r_buf.at[h, some], s_ssem.at[h], s_rsem.at[h, slot // 2], dev)
 
     def project(h):
         weights = wd_buf[h].reshape(2 * hid, wd_buf.shape[3])
@@ -482,7 +537,7 @@
 
     def join(h, slot, count, by):
         some = slice(slot + by, slot + by + count)
-        arrived(r_buf.at[h, pl.ds(slot + by, count)], s_rsem.at[h, slot + by])
+        arrived(r_buf.at[h, pl.ds(slot + by, count)], s_rsem.at[h, (slot + by) // 2])
         acc_buf[h, slot:slot + count] = (
             acc_buf[h, slot:slot + count].astype(F32) + r_buf[h, some].astype(F32)
         ).astype(BF)
@@ -504,7 +559,7 @@
         sums(h, 1, 1)
 
     def finish(h):
-        arrived(r_buf.at[h, pl.ds(1, 1)], s_rsem.at[h, 1])
+        arrived(r_buf.at[h, pl.ds(1, 1)], s_rsem.at[h, 0])
         value = acc_buf[h, 0].astype(F32) + r_buf[h, 1].astype(F32)
         for k in range(sp):
             span = slice(k * cols + h * lanes, k * cols + (h + 1) * lanes)
@@ -512,12 +567,11 @@
                 mid_buf[:, span] + 0.5 * value[:, k * lanes:(k + 1) * lanes]
             ).astype(BF)
 
-    down_part = [[(w, q) for q in range(sp)] for w in (2, 3)]
-    pass_weights(down_part[0])
+    pass_weights(2, 1)
     passed_weights(2)
     project(0)
     reduce_first(0)
-    pass_weights(down_part[1])
+    pass_weights(3, 1)
     reduce_second(0)
     passed_weights(3)
     project(1)
@@ -528,8 +582,19 @@
     reduce_third(1)
     finish(1)
 
-    for cp in sends:
-        cp.wait_send()
+    for h in range(2):
+        sent(r_buf.at[h, pl.ds(1, 2 * sp - 1)], s_ssem.at[h])
+    sent(n_buf.at[pl.ds(1, 2 * sp - 1)], a_ssem.at[0])
+    for c in range(2):
+        sent(paird_buf.at[c], m_ssem.at[c])
+        sent(crossr_buf.at[c], m_ssem.at[2 + c])
+    sent(kv_buf.at[pl.ds(1, sp - 1), core], l_ssem.at[0])
+    sent(kv_buf.at[pl.ds(1, sp - 1), core], f_ssem.at[0])
+    for kind in range(3):
+        sent(relay_buf.at[kind], y_ssem.at[kind])
+    for which in range(4):
+        sent(some_of(which, core, sp - 1), w_ssem.at[which])
+        sent(some_of(which, core, sp), x_ssem.at[which])
 
 
 def fused_layer(
@@ -575,14 +640,17 @@
             vmem(*out_weight.shape),
             vmem(part, width),
             vmem(2, *gate_weight.shape),
-            vmem(2, *gate_weight.shape[::-1]),
+            vmem(3, sp, hid, cols),
+            vmem(3, sp // 2 - 1, hid, cols),
             vmem(sp, 2, rows // 2, kv + 128),
             vmem(sp * rows, heads_width),
             vmem(sp * rows, heads_width),
             vmem(rows, heads_width),
             pltpu.VMEM((rows, width), F32),
-            vmem(tp, part, width),
-            vmem(tp, part, width),
+            vmem(2, 2, tp // 2, part, width // 2),
+            vmem(2, tp // 2, part, width // 2),
+            vmem(2, part, width // 2),
+            vmem(2, part, width // 2),
             pltpu.VMEM((part, width), F32),
             vmem(2, 2, hid, width),
             vmem(2, 2, hid, width // 2),
@@ -590,21 +658,23 @@
             vmem(chips * part, 2 * hid),
             vmem(2, chips, part, width // 2),
             vmem(2, chips, part, width // 2),
-            dma((10,)),
+            dma((11,)),
+            dma((1,)),
             dma((sp,)),
+            dma((1,)),
             dma((sp,)),
-            dma((sp,)),
-            dma((sp,)),
-            dma((tp,)),
-            dma((tp,)),
-            dma((4, sp)),
-            dma((4, sp)),
-            dma((4, sp)),
-            dma((4, sp)),
-            dma((chips,)),
-            dma((chips,)),
-            dma((2, chips)),
-            dma((2, chips)),
+            dma((4,)),
+            dma((4,)),
+            dma((4,)),
+            dma((4, 2)),
+            dma((3,)),
+            dma((3,)),
+            dma((4,)),
+            dma((4,)),
+            dma((1,)),
+            dma((sp + 1,)),
+            dma((2,)),
+            dma((2, sp)),
         ],
         compiler_params=pltpu.CompilerParams(
             collective_id=0, has_side_effects=True, vmem_limit_bytes=60 * 1024 * 1024

time: 107 us -> 99.4 us (0.929)
  Pallas kernels: 104 us -> 97 us
    pallas_call x1, Pallas kernels: 104 us -> 97 us  [fused_layer(): pl.pallas_call(functools.partial(layer_kernel, (sp, tp)), out_shape=jax.S...]
where the time goes in v2:
time: 99.4 us; the launch traced here: 99.2 us
  Pallas kernels  97 us (98%)
  local copies, waits for them, and re-layouts  2.17 us (2%)
    pallas_call x1, Pallas kernels, fused_layer(): pl.pallas_call(functools.partial(layer_kernel, (sp, tp)), out_shape=jax.S...  97 us

profile of v2, /device:TPU:0, one launch (start us, length us, event | category | flops | bytes accessed | tf_op | source)
XLA Modules:
  0.0 99.2 jit_solution(9633573036790138868)
XLA Ops:
  0.0 0.6 broadcast_in_dim_tile.3.inv_ref
  0.6 97.0 %shard_map.127 = bf16[32,2048]{1,0:T(8,128)(2,1)} custom-call(bf16[128,256]{1,0:T(8,128)(2,1)} %latent_ref.1, bf16[32,128]{1,0:T(8,128)(2,1)} %bitcast.5, f32[1,128]{1,0:T(1,128)} %broadcast_in_dim_tile.3.inv_ref, f32[1,256]{1,0:T(1,128)} %bitcast.7, f32[1,2048]{1,0:T(1,128)} %bitcast.6, bf16[128,512]{1,0:T(8,128)(2,1)} %query_hbm.1, ...), custom_call_target="tpu_custom_call" | custom-call | tf_op jit(solution)/shard_map/pallas_call | solution.py:630
  97.6 1.6 %copy.15 = bf16[32,2048]{1,0:T(8,128)(2,1)} copy(bf16[32,2048]{1,0:T(8,128)(2,1)} %shard_map.127) | data formatting | bytes 262144
  (2 shorter events, 0.0 us)

commit v3 on v2

--- a/solution.py
+++ b/solution.py
@@ -205,6 +205,8 @@
     load_sem,
     l_ssem,
     l_rsem,
+    c_ssem,
+    c_rsem,
     f_ssem,
     f_rsem,
     m_ssem,
@@ -230,11 +232,11 @@
     zh = s // 4
     other = t + 1 - 2 * core
     rows = latent_ref.shape[0]
-    half_rows = rows // 2
     part = rows // tp
     hid, cols = down_hbm.shape[1:]
     kv_width = latent_ref.shape[1]
     lanes = cols // 2
+    quarter = sp // 2 * lanes
     width = ow_hbm.shape[1]
     along_x = (s, (1 - x) * 2 + core)
 
@@ -297,10 +299,10 @@
     shared = shared_ref[...].astype(F32)
     shared = jnp.concatenate([shared] * (128 // ROPE), axis=0).T
     own_key = turn(shared, cosine, sine).astype(BF)
-    for half in range(2):
-        part_of = slice(half * half_rows, (half + 1) * half_rows)
-        kv_buf[0, half, :, :kv_width] = own_lat[part_of]
-        kv_buf[0, half, :, kv_width:] = own_key[part_of]
+    for j in range(tp):
+        part_of = slice(j * part, (j + 1) * part)
+        kv_buf[0, j, :, :kv_width] = own_lat[part_of]
+        kv_buf[0, j, :, kv_width:] = own_key[part_of]
 
     pl.semaphore_wait(barrier, sp - 1 + tp - 1)
 
@@ -308,7 +310,7 @@
 
     def send_latent(slot, by):
         to = slot + by
-        send(kv_buf.at[slot, core], kv_buf.at[to, core], l_ssem.at[0], l_rsem.at[to], (ring(by), t))
+        send(kv_buf.at[slot, t], kv_buf.at[to, t], l_ssem.at[0], l_rsem.at[to], (ring(by), t))
 
     for by in (6, 4, 2, 1):
         send_latent(0, by)
@@ -320,13 +322,21 @@
             tile = slice(j * 128, (j + 1) * 128)
             turned_buf[tile, :] = raw_buf[which, :, tile].T
 
-    first = [(0, 6), (1, 6), (0, 4), (1, 4)]
-    second = [(0, 7)]
-    third = [(1, 7), (0, 5), (1, 5), (0, 2), (1, 2), (0, 3), (1, 3)]
-    fourth = [(w, q) for w in (2, 3) for q in (6, 7, 4, 5, 2, 3)]
+    first = (
+        [(0, 2), (0, 6), (1, 2), (1, 6), (0, 4)],
+        [(0, 2), (1, 2), (0, 6), (1, 6), (0, 4), (1, 4)],
+    )
+    between = ([], [(0, 7)])
+    second = ([], [(1, 7)])
+    third = (
+        [(1, 4), (0, 3), (0, 7), (1, 3), (1, 7), (0, 5), (1, 5)],
+        [(0, 3), (1, 3), (0, 5), (1, 5)],
+    )
+    fourth = [(w, q) for w in (2, 3) for q in (2, 3, 6, 7, 4, 5)]
+    outer = zl == zh
 
     def late(which, q):
-        return int((which, q) not in first and (q != 1 or which > 1))
+        return int(q in (7, 5, 3) if which < 2 else q > 3)
 
     def weight_slot(which, lane_of, side=core):
         if which < 2:
@@ -361,6 +371,15 @@
     def relayed(kind):
         arrived(relay_buf.at[kind], y_rsem.at[kind])
 
+    def send_by_place(lists):
+        @pl.when(outer)
+        def _():
+            send_weights(lists[0])
+
+        @pl.when(jnp.logical_not(outer))
+        def _():
+            send_weights(lists[1])
+
     def some_of(which, side, count):
         if which < 2:
             return w_buf.at[which, side, :, :count * cols]
@@ -369,7 +388,7 @@
     def pass_weights(which, group):
         some = [q for q in range(1, sp) if late(which, q) == group]
         arrived(some_of(which, core, len(some)), w_rsem.at[which, group])
-        for q in some + [0] * group:
+        for q in [0] * (1 - group) + some:
             slot = weight_slot(which, ring(q))
             send(slot, slot, x_ssem.at[which], x_rsem.at[which], (s, other))
 
@@ -400,12 +419,15 @@
         jnp.concatenate([sine] * (turn_ref.shape[1] // 128), axis=1),
     ).astype(BF)
 
-    def pass_latent(slot):
-        send(kv_buf.at[slot, core], kv_buf.at[slot, core], f_ssem.at[0], f_rsem.at[slot], (s, other))
+    def pass_latent(slot, quarter):
+        piece = kv_buf.at[slot, quarter]
+        send(piece, piece, f_ssem.at[0], f_rsem.at[slot], (s, other))
 
     def take_latent(slot):
-        arrived(kv_buf.at[slot, core], l_rsem.at[slot])
-        pass_latent(slot)
+        piece = kv_buf.at[slot, t]
+        arrived(piece, l_rsem.at[slot])
+        send(piece, piece, c_ssem.at[0], c_rsem.at[slot], along_x)
+        pass_latent(slot, t)
 
     take_latent(1)
     for by in (6, 4, 2):
@@ -415,9 +437,12 @@
     order = (2, 4, 6, 3, 5, 7)
     for slot in order:
         take_latent(slot)
-    send_weights(first)
+    send_by_place(first)
     for slot in (1,) + order:
-        arrived(kv_buf.at[slot, 1 - core], f_rsem.at[slot])
+        arrived(kv_buf.at[slot, along_x[1]], c_rsem.at[slot])
+        pass_latent(slot, along_x[1])
+    for slot in (1,) + order:
+        arrived(kv_buf.at[slot, pl.ds(0, tp // 2)], f_rsem.at[slot])
         make_kv(slot)
 
     scale = (NOPE + ROPE) ** (-0.5)
@@ -445,6 +470,8 @@
             results.append(jnp.dot(expo.astype(BF), vals, preferred_element_type=F32) / total)
         att_buf[:, span] = jnp.where(lane < V, results[0], results[1]).astype(BF)
 
+    relayed(0)
+    send_by_place(between)
     span_of = [slice(c * width // 2, (c + 1) * width // 2) for c in range(2)]
     for c, span in enumerate(span_of):
         mix = jnp.dot(att_buf[...], ow_ref[:, span], preferred_element_type=F32)
@@ -485,111 +512,158 @@
                 send(n_buf.at[slot], n_buf.at[to], a_ssem.at[0], a_rsem.at[min(to, sp)], dev)
 
     spread(0)
-    relayed(0)
-    send_weights(second)
+    relayed(1)
+    send_by_place(second)
     arrived(n_buf.at[1], a_rsem.at[1])
     spread(1)
-    relayed(1)
-    send_weights(third)
+    send_by_place(third)
+    relayed(2)
+    send_weights(fourth)
     for slot in (2, 3):
         arrived(n_buf.at[slot], a_rsem.at[slot])
         spread(slot)
-    relayed(2)
-    send_weights(fourth)
-    pass_weights(0, 0)
-    pass_weights(1, 0)
     for slot in (4, 5, 6, 7):
         arrived(n_buf.at[slot], a_rsem.at[slot])
         spread(slot)
+    pass_weights(0, 0)
+    pass_weights(1, 0)
     pass_weights(0, 1)
     pass_weights(1, 1)
+    group = n_buf.shape[0] // 2
+
+    def hidden_of(side):
+        for g in range(2):
+            block = n_buf[g * group:(g + 1) * group].reshape(group * part, width)
+            gate = lax.dot_general(block, w_buf[0, side], BY_LAST, preferred_element_type=F32)
+            up = lax.dot_general(block, w_buf[1, side], BY_LAST, preferred_element_type=F32)
+            hidden = (gate / (1.0 + jnp.exp(-gate)) * up).astype(BF)
+            for k in range(group):
+                slot = k % 2 * 8 + g * 4 + k // 2 % 2 * 2 + k // 4
+                h_buf[side, slot * part:(slot + 1) * part, :] = hidden[k * part:(k + 1) * part]
+
+    arrived(n_buf.at[pl.ds(group, group)], a_rsem.at[sp])
+    hidden_of(core)
     passed_weights(0)
     passed_weights(1)
-
-    group = n_buf.shape[0] // 2
-    gate_w = w_buf[0].reshape(2 * hid, w_buf.shape[3])
-    up_w = w_buf[1].reshape(2 * hid, w_buf.shape[3])
-    for g in range(2):
-        if g:
-            arrived(n_buf.at[pl.ds(group, group)], a_rsem.at[sp])
-        block = n_buf[g * group:(g + 1) * group].reshape(group * part, n_buf.shape[2])
-        gate = lax.dot_general(block, gate_w, BY_LAST, preferred_element_type=F32)
-        up = lax.dot_general(block, up_w, BY_LAST, preferred_element_type=F32)
-        h_buf[g * group * part:(g + 1) * group * part, :] = (gate / (1.0 + jnp.exp(-gate)) * up).astype(BF)
-
-    def sums(h, slot, count):
-        by, dev = next(step for step in steps if slot >= step[0])
+    hidden_of(1 - core)
+
+    to_first, to_second, to_low, to_high = (dev for by, dev in steps)
+    messages = {
+        14: (2, to_first),
+        12: (2, to_first),
+        10: (2, to_low),
+        9: (1, to_second),
+        8: (1, to_high),
+        6: (2, to_first),
+        4: (2, to_first),
+        2: (2, to_low),
+        1: (1, to_second),
+    }
+    index_of = {slot: i for i, slot in enumerate(messages)}
+
+    def sums(q, slot):
+        count, dev = messages[slot]
         some = pl.ds(slot, count)
-        send(acc_buf.at[h, some], r_buf.at[h, some], s_ssem.at[h], s_rsem.at[h, slot // 2], dev)
+        send(acc_buf.at[q, some], r_buf.at[q, some], s_ssem.at[q], s_rsem.at[q, index_of[slot]], dev)
 
     def project(h):
-        weights = wd_buf[h].reshape(2 * hid, wd_buf.shape[3])
         for g in (1, 0):
-            down = jnp.dot(
-                h_buf[g * group * part:(g + 1) * group * part, :], weights, preferred_element_type=F32
+            span = slice(g * group * part, (g + 1) * group * part)
+            down = jnp.dot(h_buf[0, span], wd_buf[h, 0], preferred_element_type=F32) + jnp.dot(
+                h_buf[1, span], wd_buf[h, 1], preferred_element_type=F32
             )
-            acc_buf[h, g * group:(g + 1) * group] = down.astype(BF).reshape(
-                group, part, acc_buf.shape[3]
-            )
-            if g:
-                for slot in (14, 12, 10, 8):
-                    sums(h, slot, 2)
-
-    def join(h, slot, count, by):
-        some = slice(slot + by, slot + by + count)
-        arrived(r_buf.at[h, pl.ds(slot + by, count)], s_rsem.at[h, (slot + by) // 2])
-        acc_buf[h, slot:slot + count] = (
-            acc_buf[h, slot:slot + count].astype(F32) + r_buf[h, some].astype(F32)
-        ).astype(BF)
-
-    def reduce_first(h):
-        for slot in (6, 4):
-            join(h, slot, 2, 8)
-            sums(h, slot, 2)
-
-    def reduce_second(h):
-        join(h, 2, 2, 8)
-        join(h, 2, 2, 4)
-        sums(h, 2, 2)
-
-    def reduce_third(h):
-        join(h, 0, 2, 8)
-        join(h, 0, 2, 4)
-        join(h, 0, 2, 2)
-        sums(h, 1, 1)
-
-    def finish(h):
-        arrived(r_buf.at[h, pl.ds(1, 1)], s_rsem.at[h, 0])
-        value = acc_buf[h, 0].astype(F32) + r_buf[h, 1].astype(F32)
-        for k in range(sp):
-            span = slice(k * cols + h * lanes, k * cols + (h + 1) * lanes)
+            for c in range(2):
+                acc_buf[2 * h + c, g * group:(g + 1) * group] = (
+                    down[:, c * quarter:(c + 1) * quarter].astype(BF).reshape(group, part, quarter)
+                )
+            for c in range(2):
+                sums(2 * h + c, g * group + 6)
+                sums(2 * h + c, g * group + 4)
+
+    def landed(q, slot):
+        count = messages[slot][0]
+        arrived(r_buf.at[q, pl.ds(slot, count)], s_rsem.at[q, index_of[slot]])
+        return r_buf[q, slot:slot + count].astype(F32)
+
+    def join(q, to, *slots):
+        count = messages[slots[0]][0]
+        value = acc_buf[q, to:to + count].astype(F32)
+        for slot in slots:
+            value = value + landed(q, slot)
+        acc_buf[q, to:to + count] = value.astype(BF)
+
+    def to_10(q):
+        join(q, 10, 14)
+        sums(q, 10)
+
+    def to_2(q):
+        join(q, 2, 6)
+        sums(q, 2)
+
+    def to_9(q):
+        join(q, 8, 12, 10)
+        sums(q, 9)
+
+    def to_8(q):
+        join(q, 8, 9)
+        sums(q, 8)
+
+    def to_1(q):
+        join(q, 0, 4, 2)
+        sums(q, 1)
+
+    def finish(q):
+        value = acc_buf[q, 0].astype(F32) + landed(q, 1)[0] + landed(q, 8)[0]
+        h, c = q // 2, q % 2
+        for k in range(sp // 2):
+            start = (c * sp // 2 + k) * cols + h * lanes
+            span = slice(start, start + lanes)
             out_ref[:, span] = (
                 mid_buf[:, span] + 0.5 * value[:, k * lanes:(k + 1) * lanes]
             ).astype(BF)
 
+    pass_weights(2, 0)
     pass_weights(2, 1)
     passed_weights(2)
     project(0)
-    reduce_first(0)
+    to_10(0)
+    to_10(1)
+    to_2(0)
+    pass_weights(3, 0)
     pass_weights(3, 1)
-    reduce_second(0)
+    to_2(1)
+    to_9(0)
+    to_9(1)
     passed_weights(3)
     project(1)
-    reduce_third(0)
-    reduce_first(1)
-    reduce_second(1)
+    to_8(0)
+    to_8(1)
+    to_10(2)
+    to_10(3)
+    to_1(0)
+    to_1(1)
+    to_2(2)
     finish(0)
-    reduce_third(1)
+    to_9(2)
+    to_2(3)
     finish(1)
-
-    for h in range(2):
+    to_9(3)
+    to_8(2)
+    to_1(2)
+    to_8(3)
+    to_1(3)
+    finish(2)
+    finish(3)
+
+    for h in range(4):
         sent(r_buf.at[h, pl.ds(1, 2 * sp - 1)], s_ssem.at[h])
     sent(n_buf.at[pl.ds(1, 2 * sp - 1)], a_ssem.at[0])
     for c in range(2):
         sent(paird_buf.at[c], m_ssem.at[c])
         sent(crossr_buf.at[c], m_ssem.at[2 + c])
-    sent(kv_buf.at[pl.ds(1, sp - 1), core], l_ssem.at[0])
-    sent(kv_buf.at[pl.ds(1, sp - 1), core], f_ssem.at[0])
+    sent(kv_buf.at[pl.ds(1, sp - 1), 0], l_ssem.at[0])
+    sent(kv_buf.at[pl.ds(1, sp - 1), 0], c_ssem.at[0])
+    sent(kv_buf.at[pl.ds(1, sp - 1), pl.ds(0, tp // 2)], f_ssem.at[0])
     for kind in range(3):
         sent(relay_buf.at[kind], y_ssem.at[kind])
     for which in range(4):
@@ -642,7 +716,7 @@
             vmem(2, *gate_weight.shape),
             vmem(3, sp, hid, cols),
             vmem(3, sp // 2 - 1, hid, cols),
-            vmem(sp, 2, rows // 2, kv + 128),
+            vmem(sp, tp, part, kv + 128),
             vmem(sp * rows, heads_width),
             vmem(sp * rows, heads_width),
             vmem(rows, heads_width),
@@ -655,10 +729,12 @@
             vmem(2, 2, hid, width),
             vmem(2, 2, hid, width // 2),
             vmem(chips, part, width),
-            vmem(chips * part, 2 * hid),
-            vmem(2, chips, part, width // 2),
-            vmem(2, chips, part, width // 2),
+            vmem(2, chips * part, hid),
+            vmem(4, chips, part, width // 4),
+            vmem(4, chips, part, width // 4),
             dma((11,)),
+            dma((1,)),
+            dma((sp,)),
             dma((1,)),
             dma((sp,)),
             dma((1,)),
@@ -673,8 +749,8 @@
             dma((4,)),
             dma((1,)),
             dma((sp + 1,)),
-            dma((2,)),
-            dma((2, sp)),
+            dma((4,)),
+            dma((4, sp + 1)),
         ],
         compiler_params=pltpu.CompilerParams(
             collective_id=0, has_side_effects=True, vmem_limit_bytes=60 * 1024 * 1024

time: 99.4 us -> 90.6 us (0.911)
  Pallas kernels: 97 us -> 88.3 us
    pallas_call x1, Pallas kernels: 97 us -> 88.3 us  [fused_layer(): pl.pallas_call(functools.partial(layer_kernel, (sp, tp)), out_shape=jax.S...]
where the time goes in v3:
time: 90.6 us; the launch traced here: 90.4 us
  Pallas kernels  88.3 us (97%)
  local copies, waits for them, and re-layouts  2.17 us (2%)
    pallas_call x1, Pallas kernels, fused_layer(): pl.pallas_call(functools.partial(layer_kernel, (sp, tp)), out_shape=jax.S...  88.3 us

profile of v3, /device:TPU:0, one launch (start us, length us, event | category | flops | bytes accessed | tf_op | source)
XLA Modules:
  0.0 90.4 jit_solution(2256886127764453481)
XLA Ops:
  0.0 0.6 broadcast_in_dim_tile.3.inv_ref
  0.6 88.3 %shard_map.127 = bf16[32,2048]{1,0:T(8,128)(2,1)} custom-call(bf16[128,256]{1,0:T(8,128)(2,1)} %latent_ref.1, bf16[32,128]{1,0:T(8,128)(2,1)} %bitcast.5, f32[1,128]{1,0:T(1,128)} %broadcast_in_dim_tile.3.inv_ref, f32[1,256]{1,0:T(1,128)} %bitcast.7, f32[1,2048]{1,0:T(1,128)} %bitcast.6, bf16[128,512]{1,0:T(8,128)(2,1)} %query_hbm.1, ...), custom_call_target="tpu_custom_call" | custom-call | tf_op jit(solution)/shard_map/pallas_call | solution.py:704
  88.9 1.6 %copy.15 = bf16[32,2048]{1,0:T(8,128)(2,1)} copy(bf16[32,2048]{1,0:T(8,128)(2,1)} %shard_map.127) | data formatting | bytes 262144
  (2 shorter events, 0.0 us)

commit v4 on v3

--- a/solution.py
+++ b/solution.py
@@ -263,6 +263,8 @@
         pl.semaphore_signal(barrier, inc=1, device_id=(ring(q), t), device_id_type=MESH)
     for j in range(1, tp):
         pl.semaphore_signal(barrier, inc=1, device_id=(s, (t + j) % tp), device_id_type=MESH)
+    for q in (2, 4):
+        pl.semaphore_signal(barrier, inc=1, device_id=(ring(q), along_x[1]), device_id_type=MESH)
 
     own_rows = pl.ds(pl.multiple_of(t * part, part), part)
     own_cols = pl.ds(pl.multiple_of(s * cols, cols), cols)
@@ -304,7 +306,7 @@
         kv_buf[0, j, :, :kv_width] = own_lat[part_of]
         kv_buf[0, j, :, kv_width:] = own_key[part_of]
 
-    pl.semaphore_wait(barrier, sp - 1 + tp - 1)
+    pl.semaphore_wait(barrier, sp - 1 + tp + 1)
 
     along_y = (ring(1), t)
 
@@ -438,14 +440,20 @@
     for slot in order:
         take_latent(slot)
     send_by_place(first)
-    for slot in (1,) + order:
+    def take_block(slot):
+        arrived(kv_buf.at[slot, pl.ds(0, tp // 2)], f_rsem.at[slot])
+        make_kv(slot)
+
+    order = (1,) + order
+    for i, slot in enumerate(order):
         arrived(kv_buf.at[slot, along_x[1]], c_rsem.at[slot])
         pass_latent(slot, along_x[1])
-    for slot in (1,) + order:
-        arrived(kv_buf.at[slot, pl.ds(0, tp // 2)], f_rsem.at[slot])
-        make_kv(slot)
-
-    scale = (NOPE + ROPE) ** (-0.5)
+        if i > 1:
+            take_block(order[i - 2])
+    for slot in order[-2:]:
+        take_block(slot)
+
+    scale = (NOPE + ROPE) ** (-0.5) * math.log2(math.e)
     all_rot = kv_buf[...].reshape(sp * rows, kv_buf.shape[3])[:, kv_width:]
     lane = lax.broadcasted_iota(jnp.int32, (rows, 128), 1)
     for pair in range(query_ref.shape[1] // 128):
@@ -463,9 +471,9 @@
             )
             score = lax.dot_general(
                 jnp.concatenate([q_plain, q_turn], axis=1), keys, BY_LAST, preferred_element_type=F32
-            ) * scale
+            )
             top = jnp.max(score, axis=-1, keepdims=True)
-            expo = jnp.exp(score - top)
+            expo = jnp.exp2((score - top) * scale)
             total = jnp.sum(expo, axis=-1, keepdims=True)
             results.append(jnp.dot(expo.astype(BF), vals, preferred_element_type=F32) / total)
         att_buf[:, span] = jnp.where(lane < V, results[0], results[1]).astype(BF)
@@ -547,6 +555,7 @@
     passed_weights(1)
     hidden_of(1 - core)
 
+    last = (3,)
     to_first, to_second, to_low, to_high = (dev for by, dev in steps)
     messages = {
         14: (2, to_first),
@@ -559,10 +568,18 @@
         2: (2, to_low),
         1: (1, to_second),
     }
-    index_of = {slot: i for i, slot in enumerate(messages)}
+    index_of = {slot: i for i, slot in enumerate((*messages, 3))}
+
+    def over(q):
+        return (ring(q + 1 - core), t + core * (along_x[1] - t))
+
+    direct = {**messages, 3: (1, over(2)), 2: (1, to_low), 9: (1, over(4))}
+
+    def message(q, slot):
+        return direct[slot] if q in last else messages[slot]
 
     def sums(q, slot):
-        count, dev = messages[slot]
+        count, dev = message(q, slot)
         some = pl.ds(slot, count)
         send(acc_buf.at[q, some], r_buf.at[q, some], s_ssem.at[q], s_rsem.at[q, index_of[slot]], dev)
 
@@ -581,12 +598,12 @@
                 sums(2 * h + c, g * group + 4)
 
     def landed(q, slot):
-        count = messages[slot][0]
+        count = message(q, slot)[0]
         arrived(r_buf.at[q, pl.ds(slot, count)], s_rsem.at[q, index_of[slot]])
         return r_buf[q, slot:slot + count].astype(F32)
 
     def join(q, to, *slots):
-        count = messages[slots[0]][0]
+        count = message(q, slots[0])[0]
         value = acc_buf[q, to:to + count].astype(F32)
         for slot in slots:
             value = value + landed(q, slot)
@@ -598,22 +615,29 @@
 
     def to_2(q):
         join(q, 2, 6)
+        if q in last:
+            sums(q, 3)
         sums(q, 2)
 
     def to_9(q):
         join(q, 8, 12, 10)
         sums(q, 9)
+        if q in last:
+            sums(q, 8)
 
     def to_8(q):
-        join(q, 8, 9)
-        sums(q, 8)
+        if q not in last:
+            join(q, 8, 9)
+            sums(q, 8)
 
     def to_1(q):
-        join(q, 0, 4, 2)
+        join(q, 0, *((4,) if q in last else (4, 2)))
         sums(q, 1)
 
     def finish(q):
-        value = acc_buf[q, 0].astype(F32) + landed(q, 1)[0] + landed(q, 8)[0]
+        value = acc_buf[q, 0].astype(F32)
+        for slot in (2, 3, 9, 1, 8) if q in last else (1, 8):
+            value = value + landed(q, slot)[0]
         h, c = q // 2, q % 2
         for k in range(sp // 2):
             start = (c * sp // 2 + k) * cols + h * lanes
@@ -643,14 +667,13 @@
     to_1(0)
     to_1(1)
     to_2(2)
-    finish(0)
     to_9(2)
     to_2(3)
-    finish(1)
+    finish(0)
     to_9(3)
     to_8(2)
     to_1(2)
-    to_8(3)
+    finish(1)
     to_1(3)
     finish(2)
     finish(3)
@@ -703,7 +726,7 @@
     far = pl.BlockSpec(memory_space=pl.ANY)
     return pl.pallas_call(
         functools.partial(layer_kernel, (sp, tp)),
-        out_shape=jax.ShapeDtypeStruct((part, width), BF),
+        out_shape=pltpu.VMEM((part, width), BF),
         in_specs=[near] * 5 + [far] * 9,
         out_specs=near,
         scratch_shapes=[
@@ -750,7 +773,7 @@
             dma((1,)),
             dma((sp + 1,)),
             dma((4,)),
-            dma((4, sp + 1)),
+            dma((4, sp + 2)),
         ],
         compiler_params=pltpu.CompilerParams(
             collective_id=0, has_side_effects=True, vmem_limit_bytes=60 * 1024 * 1024

time: 90.6 us -> 87.1 us (0.961)
  Pallas kernels: 88.3 us -> 85.7 us
  local copies, waits for them, and re-layouts: 2.17 us -> 1.26 us
    pallas_call x1, Pallas kernels: 88.3 us -> 85.7 us  [fused_layer(): pl.pallas_call(functools.partial(layer_kernel, (sp, tp)), out_shape=pltpu...]
    unnamed x1, local copies, waits for them, and re-layouts: 1.57 us -> 0.66 us
where the time goes in v4:
time: 87.1 us; the launch traced here: 87 us
  Pallas kernels  85.7 us (98%)
  local copies, waits for them, and re-layouts  1.26 us (1%)
    pallas_call x1, Pallas kernels, fused_layer(): pl.pallas_call(functools.partial(layer_kernel, (sp, tp)), out_shape=pltpu...  85.7 us

profile of v4, /device:TPU:0, one launch (start us, length us, event | category | flops | bytes accessed | tf_op | source)
XLA Modules:
  0.0 87.0 jit_solution(4199881568579243826)
XLA Ops:
  0.0 0.6 broadcast_in_dim_tile.3.inv_ref
  0.6 85.7 %shard_map.127 = bf16[32,2048]{1,0:T(8,128)(2,1)S(1)} custom-call(bf16[128,256]{1,0:T(8,128)(2,1)} %latent_ref.1, bf16[32,128]{1,0:T(8,128)(2,1)} %bitcast.5, f32[1,128]{1,0:T(1,128)} %broadcast_in_dim_tile.3.inv_ref, f32[1,256]{1,0:T(1,128)} %bitcast.7, f32[1,2048]{1,0:T(1,128)} %bitcast.6, bf16[128,512]{1,0:T(8,128)(2,1)} %query_hbm.1, ...), custom_call_target="tpu_custom_call" | custom-call | tf_op jit(solution)/shard_map/pallas_call | solution.py:727
  86.3 0.7 copy.15
  (2 shorter events, 0.0 us)

commit v5 on v4

--- a/solution.py
+++ b/solution.py
@@ -240,9 +240,17 @@
     width = ow_hbm.shape[1]
     along_x = (s, (1 - x) * 2 + core)
 
+    def bits(q):
+        flip = lambda bit, by: bit + by * (1 - 2 * bit)
+        return flip(zh, q // 4), flip(zl, q // 2 % 2), flip(y, q % 2)
+
     def ring(q):
-        flip = lambda bit, by: bit + by * (1 - 2 * bit)
-        return flip(zh, q // 4) * 4 + flip(zl, q // 2 % 2) * 2 + flip(y, q % 2)
+        high, low, side = bits(q)
+        return high * 4 + low * 2 + side
+
+    def place(q):
+        high, low, side = bits(q)
+        return (1 - high - low + 2 * high * low) * 4 + high * 2 + side
 
     def remote(src, dst, ssem, rsem, dev):
         return pltpu.make_async_remote_copy(
@@ -268,7 +276,7 @@
 
     own_rows = pl.ds(pl.multiple_of(t * part, part), part)
     own_cols = pl.ds(pl.multiple_of(s * cols, cols), cols)
-    own_lanes = pl.ds(pl.multiple_of(s * lanes, lanes), lanes)
+    own_lanes = pl.ds(pl.multiple_of(place(0) * lanes, lanes), lanes)
     loads = [
         pltpu.make_async_copy(src, dst, load_sem.at[i])
         for i, (src, dst) in enumerate(
@@ -335,15 +343,16 @@
         [(0, 3), (1, 3), (0, 5), (1, 5)],
     )
     fourth = [(w, q) for w in (2, 3) for q in (2, 3, 6, 7, 4, 5)]
-    outer = zl == zh
+    role = 1 - zh - zl + 2 * zh * zl
+    outer = role == 1
 
     def late(which, q):
-        return int(q in (7, 5, 3) if which < 2 else q > 3)
-
-    def weight_slot(which, lane_of, side=core):
+        return int(q in (7, 5, 3)) if which < 2 else role
+
+    def weight_slot(which, q, side=core):
         if which < 2:
-            return w_buf.at[which, side, :, pl.ds(pl.multiple_of(lane_of * cols, cols), cols)]
-        return wd_buf.at[which - 2, side, :, pl.ds(pl.multiple_of(lane_of * lanes, lanes), lanes)]
+            return w_buf.at[which, side, :, pl.ds(pl.multiple_of(ring(q) * cols, cols), cols)]
+        return wd_buf.at[which - 2, side, :, pl.ds(pl.multiple_of(place(q) * lanes, lanes), lanes)]
 
     def lanes_of(ref, which):
         return ref if which < 2 else ref.at[:, (which - 2) * lanes:(which - 1) * lanes]
@@ -352,9 +361,9 @@
         for which, q in some:
             kind = min(which, 2)
             if q > 1 and q % 2:
-                src, owner, dest = relay_buf.at[kind, q // 2 - 1], ring(1), (ring(q - 1), t)
+                src, owner, dest = relay_buf.at[kind, q // 2 - 1], 1, (ring(q - 1), t)
             else:
-                src, owner, dest = wt_buf.at[kind, ring(q)], s, (ring(q), t)
+                src, owner, dest = wt_buf.at[kind, ring(q)], 0, (ring(q), t)
             send(
                 lanes_of(src, which),
                 weight_slot(which, owner),
@@ -387,15 +396,34 @@
             return w_buf.at[which, side, :, :count * cols]
         return wd_buf.at[which - 2, side, :, :count * lanes]
 
+    def pass_on(which, some, index):
+        for q in some:
+            slot = weight_slot(which, q)
+            send(slot, slot, x_ssem.at[index], x_rsem.at[index], (s, other))
+
     def pass_weights(which, group):
         some = [q for q in range(1, sp) if late(which, q) == group]
         arrived(some_of(which, core, len(some)), w_rsem.at[which, group])
-        for q in [0] * (1 - group) + some:
-            slot = weight_slot(which, ring(q))
-            send(slot, slot, x_ssem.at[which], x_rsem.at[which], (s, other))
+        pass_on(which, [0] * (1 - group) + some, which)
 
     def passed_weights(which):
         arrived(some_of(which, 1 - core, sp), x_rsem.at[which])
+
+    def pass_down(q):
+        h, c = q // 2, q % 2
+
+        @pl.when(role == c)
+        def _():
+            arrived(some_of(2 + h, core, sp // 2 - 1), w_rsem.at[2 + h, c])
+            pass_on(2 + h, (0, 1, 6, 7), 2 + q)
+
+        @pl.when(role != c)
+        def _():
+            arrived(some_of(2 + h, core, sp // 2), w_rsem.at[2 + h, c])
+            pass_on(2 + h, (2, 3, 4, 5), 2 + q)
+
+    def passed_down(q):
+        arrived(some_of(2 + q // 2, 1 - core, sp // 2), x_rsem.at[2 + q])
 
     send_relays(0)
     send_relays(1)
@@ -583,19 +611,16 @@
         some = pl.ds(slot, count)
         send(acc_buf.at[q, some], r_buf.at[q, some], s_ssem.at[q], s_rsem.at[q, index_of[slot]], dev)
 
-    def project(h):
+    def project(q):
+        h, columns = q // 2, slice(q % 2 * quarter, (q % 2 + 1) * quarter)
         for g in (1, 0):
             span = slice(g * group * part, (g + 1) * group * part)
-            down = jnp.dot(h_buf[0, span], wd_buf[h, 0], preferred_element_type=F32) + jnp.dot(
-                h_buf[1, span], wd_buf[h, 1], preferred_element_type=F32
-            )
-            for c in range(2):
-                acc_buf[2 * h + c, g * group:(g + 1) * group] = (
-                    down[:, c * quarter:(c + 1) * quarter].astype(BF).reshape(group, part, quarter)
-                )
-            for c in range(2):
-                sums(2 * h + c, g * group + 6)
-                sums(2 * h + c, g * group + 4)
+            down = jnp.dot(
+                h_buf[0, span], wd_buf[h, 0, :, columns], preferred_element_type=F32
+            ) + jnp.dot(h_buf[1, span], wd_buf[h, 1, :, columns], preferred_element_type=F32)
+            acc_buf[q, g * group:(g + 1) * group] = down.astype(BF).reshape(group, part, quarter)
+            sums(q, g * group + 6)
+            sums(q, g * group + 4)
 
     def landed(q, slot):
         count = message(q, slot)[0]
@@ -640,41 +665,46 @@
             value = value + landed(q, slot)[0]
         h, c = q // 2, q % 2
         for k in range(sp // 2):
-            start = (c * sp // 2 + k) * cols + h * lanes
+            z = (1 + k // 2) if c == 0 else 3 * (k // 2)
+            start = (2 * z + k % 2) * cols + h * lanes
             span = slice(start, start + lanes)
             out_ref[:, span] = (
                 mid_buf[:, span] + 0.5 * value[:, k * lanes:(k + 1) * lanes]
             ).astype(BF)
 
-    pass_weights(2, 0)
-    pass_weights(2, 1)
-    passed_weights(2)
+    pass_down(0)
+    passed_down(0)
     project(0)
+    pass_down(1)
+    passed_down(1)
+    project(1)
     to_10(0)
+    to_2(0)
+    pass_down(2)
+    passed_down(2)
+    project(2)
     to_10(1)
-    to_2(0)
-    pass_weights(3, 0)
-    pass_weights(3, 1)
+    to_9(0)
     to_2(1)
-    to_9(0)
+    pass_down(3)
+    passed_down(3)
+    project(3)
     to_9(1)
-    passed_weights(3)
-    project(1)
+    to_10(2)
+    to_2(2)
     to_8(0)
+    to_10(3)
     to_8(1)
-    to_10(2)
-    to_10(3)
+    to_9(2)
+    to_2(3)
     to_1(0)
     to_1(1)
-    to_2(2)
-    to_9(2)
-    to_2(3)
+    to_8(2)
+    to_9(3)
+    to_1(2)
+    to_1(3)
     finish(0)
-    to_9(3)
-    to_8(2)
-    to_1(2)
     finish(1)
-    to_1(3)
     finish(2)
     finish(3)
 
@@ -691,7 +721,10 @@
         sent(relay_buf.at[kind], y_ssem.at[kind])
     for which in range(4):
         sent(some_of(which, core, sp - 1), w_ssem.at[which])
+    for which in range(2):
         sent(some_of(which, core, sp), x_ssem.at[which])
+        for c in range(2):
+            sent(some_of(2 + which, core, sp // 2), x_ssem.at[2 + 2 * which + c])
 
 
 def fused_layer(
@@ -768,8 +801,8 @@
             dma((4, 2)),
             dma((3,)),
             dma((3,)),
-            dma((4,)),
-            dma((4,)),
+            dma((6,)),
+            dma((6,)),
             dma((1,)),
             dma((sp + 1,)),
             dma((4,)),

time: 87.1 us -> 86.3 us (level)
  Pallas kernels: 85.7 us -> 84.8 us
where the time goes in v5:
time: 86.3 us; the launch traced here: 86.1 us
  Pallas kernels  84.8 us (98%)
  local copies, waits for them, and re-layouts  1.26 us (1%)
    pallas_call x1, Pallas kernels, fused_layer(): pl.pallas_call(functools.partial(layer_kernel, (sp, tp)), out_shape=pltpu...  84.8 us

profile of v5, /device:TPU:0, one launch (start us, length us, event | category | flops | bytes accessed | tf_op | source)
XLA Modules:
  0.0 86.1 jit_solution(4868870408090181509)
XLA Ops:
  0.0 0.6 broadcast_in_dim_tile.3.inv_ref
  0.6 84.8 %shard_map.127 = bf16[32,2048]{1,0:T(8,128)(2,1)S(1)} custom-call(bf16[128,256]{1,0:T(8,128)(2,1)} %latent_ref.1, bf16[32,128]{1,0:T(8,128)(2,1)} %bitcast.5, f32[1,128]{1,0:T(1,128)} %broadcast_in_dim_tile.3.inv_ref, f32[1,256]{1,0:T(1,128)} %bitcast.7, f32[1,2048]{1,0:T(1,128)} %bitcast.6, bf16[128,512]{1,0:T(8,128)(2,1)} %query_hbm.1, ...), custom_call_target="tpu_custom_call" | custom-call | tf_op jit(solution)/shard_map/pallas_call | solution.py:760
  85.5 0.7 copy.15
  (2 shorter events, 0.0 us)

commit v6 on v5

--- a/solution.py
+++ b/solution.py
@@ -367,7 +367,7 @@
             send(
                 lanes_of(src, which),
                 weight_slot(which, owner),
-                w_ssem.at[which],
+                w_ssem.at[which // 2],
                 w_rsem.at[which, late(which, q)],
                 dest,
             )
@@ -375,7 +375,7 @@
     def send_relays(kind):
         for q in (7, 5, 3):
             send(
-                wt_buf.at[kind, ring(q)], relay_buf.at[kind, q // 2 - 1], y_ssem.at[kind], y_rsem.at[kind], along_y
+                wt_buf.at[kind, ring(q)], relay_buf.at[kind, q // 2 - 1], y_ssem.at[0], y_rsem.at[kind], along_y
             )
         send_weights([(which, 1) for which in ((kind,) if kind < 2 else (2, 3))])
 
@@ -399,7 +399,7 @@
     def pass_on(which, some, index):
         for q in some:
             slot = weight_slot(which, q)
-            send(slot, slot, x_ssem.at[index], x_rsem.at[index], (s, other))
+            send(slot, slot, x_ssem.at[which // 2], x_rsem.at[index], (s, other))
 
     def pass_weights(which, group):
         some = [q for q in range(1, sp) if late(which, q) == group]
@@ -514,12 +514,12 @@
         mix_buf[:, span] = mix
         for dest in range(tp):
             pair_buf[dest % 2, c, dest // 2] = mix[dest * part:(dest + 1) * part].astype(BF)
-        send(pair_buf.at[1 - core, c], paird_buf.at[c], m_ssem.at[c], m_rsem.at[c], (s, other))
+        send(pair_buf.at[1 - core, c], paird_buf.at[c], m_ssem.at[0], m_rsem.at[c], (s, other))
     cross_rows = pl.ds(pl.multiple_of(((1 - x) * 2 + core) * part, part), part)
     for c, span in enumerate(span_of):
         arrived(paird_buf.at[c], m_rsem.at[c])
         cross_buf[c] = (mix_buf[cross_rows, span] + paird_buf[c, 1 - x].astype(F32)).astype(BF)
-        send(cross_buf.at[c], crossr_buf.at[c], m_ssem.at[2 + c], m_rsem.at[2 + c], along_x)
+        send(cross_buf.at[c], crossr_buf.at[c], m_ssem.at[1], m_rsem.at[2 + c], along_x)
     mids = [
         resid_ref[:, span].astype(F32) + mix_buf[own_rows, span] + paird_buf[c, x].astype(F32)
         for c, span in enumerate(span_of)
@@ -609,7 +609,7 @@
     def sums(q, slot):
         count, dev = message(q, slot)
         some = pl.ds(slot, count)
-        send(acc_buf.at[q, some], r_buf.at[q, some], s_ssem.at[q], s_rsem.at[q, index_of[slot]], dev)
+        send(acc_buf.at[q, some], r_buf.at[q, some], s_ssem.at[0], s_rsem.at[q, index_of[slot]], dev)
 
     def project(q):
         h, columns = q // 2, slice(q % 2 * quarter, (q % 2 + 1) * quarter)
@@ -708,23 +708,19 @@
     finish(2)
     finish(3)
 
-    for h in range(4):
-        sent(r_buf.at[h, pl.ds(1, 2 * sp - 1)], s_ssem.at[h])
+    rest = pl.ds(1, sp - 1)
+    sent(r_buf.at[:, pl.ds(1, 2 * sp - 1)], s_ssem.at[0])
     sent(n_buf.at[pl.ds(1, 2 * sp - 1)], a_ssem.at[0])
-    for c in range(2):
-        sent(paird_buf.at[c], m_ssem.at[c])
-        sent(crossr_buf.at[c], m_ssem.at[2 + c])
-    sent(kv_buf.at[pl.ds(1, sp - 1), 0], l_ssem.at[0])
-    sent(kv_buf.at[pl.ds(1, sp - 1), 0], c_ssem.at[0])
-    sent(kv_buf.at[pl.ds(1, sp - 1), pl.ds(0, tp // 2)], f_ssem.at[0])
-    for kind in range(3):
-        sent(relay_buf.at[kind], y_ssem.at[kind])
-    for which in range(4):
-        sent(some_of(which, core, sp - 1), w_ssem.at[which])
-    for which in range(2):
-        sent(some_of(which, core, sp), x_ssem.at[which])
-        for c in range(2):
-            sent(some_of(2 + which, core, sp // 2), x_ssem.at[2 + 2 * which + c])
+    sent(paird_buf, m_ssem.at[0])
+    sent(crossr_buf, m_ssem.at[1])
+    sent(kv_buf.at[rest, 0], l_ssem.at[0])
+    sent(kv_buf.at[rest, 0], c_ssem.at[0])
+    sent(kv_buf.at[rest, pl.ds(0, tp // 2)], f_ssem.at[0])
+    sent(relay_buf, y_ssem.at[0])
+    sent(w_buf.at[:, 0, :, :(sp - 1) * cols], w_ssem.at[0])
+    sent(wd_buf.at[:, 0, :, :(sp - 1) * lanes], w_ssem.at[1])
+    sent(w_buf.at[:, 0], x_ssem.at[0])
+    sent(wd_buf.at[:, 0], x_ssem.at[1])
 
 
 def fused_layer(
@@ -795,17 +791,17 @@
             dma((sp,)),
             dma((1,)),
             dma((sp,)),
+            dma((2,)),
             dma((4,)),
-            dma((4,)),
-            dma((4,)),
+            dma((2,)),
             dma((4, 2)),
+            dma((1,)),
             dma((3,)),
-            dma((3,)),
-            dma((6,)),
+            dma((2,)),
             dma((6,)),
             dma((1,)),
             dma((sp + 1,)),
-            dma((4,)),
+            dma((1,)),
             dma((4, sp + 2)),
         ],
         compiler_params=pltpu.CompilerParams(

time: 86.3 us -> 86.1 us (level)
  no operation moved by 1% of the time
where the time goes in v6:
time: 86.1 us; the launch traced here: 86 us
  Pallas kernels  84.7 us (98%)
  local copies, waits for them, and re-layouts  1.26 us (1%)
    pallas_call x1, Pallas kernels, fused_layer(): pl.pallas_call(functools.partial(layer_kernel, (sp, tp)), out_shape=pltpu...  84.7 us

profile of v6, /device:TPU:0, one launch (start us, length us, event | category | flops | bytes accessed | tf_op | source)
XLA Modules:
  0.0 86.0 jit_solution(1078699377645270839)
XLA Ops:
  0.0 0.6 broadcast_in_dim_tile.3.inv_ref
  0.6 84.7 %shard_map.127 = bf16[32,2048]{1,0:T(8,128)(2,1)S(1)} custom-call(bf16[128,256]{1,0:T(8,128)(2,1)} %latent_ref.1, bf16[32,128]{1,0:T(8,128)(2,1)} %bitcast.5, f32[1,128]{1,0:T(1,128)} %broadcast_in_dim_tile.3.inv_ref, f32[1,256]{1,0:T(1,128)} %bitcast.7, f32[1,2048]{1,0:T(1,128)} %bitcast.6, bf16[128,512]{1,0:T(8,128)(2,1)} %query_hbm.1, ...), custom_call_target="tpu_custom_call" | custom-call | tf_op jit(solution)/shard_map/pallas_call | solution.py:756
  85.3 0.7 copy.15
  (2 shorter events, 0.0 us)
